TPU v7x, 128 devices: a whole 4x4x4 slice. The times are simulated.
128 devices in a mesh: sp: 16 (over z, x), tp: 8 (over y, core).
Axes of the slice: x: 4, y: 4, z: 4, core: 2. Of those that a mesh axis runs over, the one named last changes fastest.
Arguments:
- latent: bfloat16 [12288, 2048], P(('sp', 'tp')), may hold values from -6 to 6
- context: bfloat16 [1024, 2048], P('sp'), may hold values from -6 to 6
- conditioning: float32 [2, 2048], replicated, may hold values from -6 to 6
- norm_gain: float32 [2048], replicated, may hold values from 0.1 to 1.9
- mod_shift: bfloat16 [2048, 2048], P('sp', 'tp'), may hold values from -0.1875 to 0.1875
- mod_scale: bfloat16 [2048, 2048], P('sp', 'tp'), may hold values from -0.1875 to 0.1875
- mod_gate: bfloat16 [2048, 2048], P('sp', 'tp'), may hold values from -0.1875 to 0.1875
- w_query: bfloat16 [2048, 2048], P(None, 'tp'), may hold values from -4 to 4
- w_key: bfloat16 [2048, 2048], P(None, 'tp'), may hold values from -0.125 to 0.125
- w_value: bfloat16 [2048, 2048], P(None, 'tp'), may hold values from -0.125 to 0.125
- w_out: bfloat16 [2048, 2048], P('tp'), may hold values from -0.125 to 0.125
- lambdas: float32 [16], P('tp'), may hold values from 0.3 to 0.8
- context_bias: float32 [16], P('tp'), may hold values from 0.8 to 2.2
- head_gain: float32 [128], replicated, may hold values from 0.1 to 1.9
Outputs:
- updated: bfloat16 [12288, 2048], P(('sp', 'tp'))
All inputs are finite; a program needn't handle non-finite values.
Results may differ from a plain program's by a relative error of at most 0.01.
The roundings to bfloat16 on the way count: a program that leaves them out, or rounds other values in their place, can miss the bound.
Values may be sent and summed in bfloat16 or wider, within the bound.
A program may use at most 128 MiB of HBM per device.

v0:
```python
import jax
import jax.numpy as jnp
from jax import lax
from jax.sharding import PartitionSpec as P

EPS = 1e-06
NEGATIVE = -1e30


def copy_for_each(shard, axis):
    count = lax.axis_size(axis)
    return lax.all_to_all(
        jnp.broadcast_to(shard[None], (count, *shard.shape)), axis, 0, 0, tiled=True
    )


def of_everyone(shard, axis):
    return copy_for_each(shard, axis).sum(axis=0)


def joined_along(parts, dim):
    parts = jnp.moveaxis(parts, 0, dim)
    dims = parts.shape
    return parts.reshape(*dims[:dim], dims[dim] * dims[dim + 1], *dims[dim + 2 :])


def gathered_copies(shard, axis, dim):
    return joined_along(copy_for_each(shard, axis), dim)


def modulated(inputs, norm_scale, offset_vec, scale_vec):
    rows_float = inputs.astype(jnp.float32)
    normal = rows_float * lax.rsqrt(jnp.mean(rows_float * rows_float, axis=-1, keepdims=True) + EPS)
    return (normal * norm_scale * (1.0 + scale_vec) + offset_vec).astype(jnp.bfloat16)


def block_size(length):
    for candidate in range(min(length, 1024), 0, -1):
        if length % candidate == 0:
            return candidate
    return length


def absorb(running, portion, context_flags, queries, bias_heads):
    head_count = queries.shape[1]
    head_dim = queries.shape[3]
    row_count = portion.shape[0]
    head_cols = head_count * 2 * head_dim
    key_rows = portion[:, :head_cols].reshape(row_count, head_count, 2, head_dim)
    value_rows = portion[:, head_cols:].reshape(row_count, head_count, 2 * head_dim)
    shifts = bias_heads[:, None, None] * context_flags[None, None, :]
    updated = []
    for which_map in range(2):
        previous, weight, accumulated = running[3 * which_map : 3 * which_map + 3]
        scores = (
            jnp.einsum(
                "qhd,khd->hqk",
                queries[:, :, which_map],
                key_rows[:, :, which_map],
                preferred_element_type=jnp.float32,
            )
            * head_dim ** (-0.5)
            + shifts
        )
        peak_new = jnp.maximum(previous, jnp.max(scores, axis=2))
        faded = jnp.exp(previous - peak_new)
        raised = jnp.exp(scores - peak_new[:, :, None])
        weight = weight * faded + jnp.sum(raised, axis=2)
        accumulated = accumulated * faded.T[:, :, None] + jnp.einsum(
            "hqk,khd->qhd",
            raised.astype(jnp.bfloat16),
            value_rows,
            preferred_element_type=jnp.float32,
        )
        updated += [peak_new, weight, accumulated]
    return tuple(updated)


def absorb_rows(running, portion, context_flags, queries, bias_heads):
    row_count = portion.shape[0]
    block_len = block_size(row_count)
    if block_len == row_count:
        return absorb(running, portion, context_flags, queries, bias_heads)
    stacked = portion.reshape(row_count // block_len, block_len, portion.shape[1])
    flag_blocks = context_flags.reshape(row_count // block_len, block_len)

    def advance(state_now, operand):
        return (absorb(state_now, operand[0], operand[1], queries, bias_heads), None)

    running, unused = lax.scan(advance, running, (stacked, flag_blocks))
    return running


def per_device(
    latent,
    context,
    conditioning,
    norm_gain,
    mod_shift,
    mod_scale,
    mod_gate,
    w_query,
    w_key,
    w_value,
    w_out,
    lambdas,
    context_bias,
    head_gain,
):
    head_dim = head_gain.shape[0] // 2
    head_count = lambdas.shape[0]
    rows_sp = mod_shift.shape[0]
    cond_rows = lax.dynamic_slice_in_dim(conditioning, lax.axis_index("sp") * rows_sp, rows_sp, 1)
    activated = jax.nn.silu(cond_rows).astype(jnp.bfloat16)
    partials = jnp.stack(
        [
            jnp.dot(activated, matrix, preferred_element_type=jnp.float32)
            for matrix in (mod_shift, mod_scale, mod_gate)
        ],
        axis=1,
    )
    summed = of_everyone(partials, "sp")
    modulation = gathered_copies(summed, "tp", 2)
    own_rows = modulated(latent, norm_gain, modulation[0, 0], modulation[0, 1])
    context_rows = modulated(context, norm_gain, modulation[1, 0], modulation[1, 1])
    key_value = jnp.concatenate([w_key, w_value], axis=1)
    projector = jnp.concatenate([w_query, key_value], axis=1)
    projected = jnp.dot(
        lax.all_gather(own_rows, "tp", axis=0, tiled=True),
        projector,
        preferred_element_type=jnp.float32,
    ).astype(jnp.bfloat16)
    head_cols = w_query.shape[1]
    token_count = projected.shape[0]
    queries = projected[:, :head_cols].reshape(token_count, head_count, 2, head_dim)
    latent_kv = projected[:, head_cols:]
    context_kv = jnp.dot(context_rows, key_value, preferred_element_type=jnp.float32).astype(
        jnp.bfloat16
    )
    first_map = (
        jnp.full((head_count, token_count), NEGATIVE, jnp.float32),
        jnp.zeros((head_count, token_count), jnp.float32),
        jnp.zeros((token_count, head_count, 2 * head_dim), jnp.float32),
    )
    initial = first_map + first_map
    every_context = gathered_copies(context_kv, "sp", 0)
    running = absorb_rows(
        initial,
        every_context,
        jnp.ones((every_context.shape[0],), jnp.float32),
        queries,
        context_bias,
    )
    portion = lax.all_gather(latent_kv, "sp", axis=0, tiled=True)
    running = absorb_rows(
        running, portion, jnp.zeros((portion.shape[0],), jnp.float32), queries, context_bias
    )
    peak_one, total_one, accum_one, peak_two, total_two, accum_two = running
    mixed = accum_one / total_one.T[:, :, None] - lambdas[None, :, None] * (
        accum_two / total_two.T[:, :, None]
    )
    normed = mixed * lax.rsqrt(jnp.mean(mixed * mixed, axis=-1, keepdims=True) + EPS) * head_gain
    flattened = normed.reshape(token_count, head_cols).astype(jnp.bfloat16)
    attended = lax.psum_scatter(
        jnp.dot(flattened, w_out, preferred_element_type=jnp.float32).astype(jnp.bfloat16),
        "tp",
        scatter_dimension=0,
        tiled=True,
    )
    return (latent.astype(jnp.float32) + modulation[0, 2] * attended.astype(jnp.float32)).astype(
        jnp.bfloat16
    )


def solution(mesh):
    return jax.shard_map(
        per_device,
        mesh=mesh,
        in_specs=(
            P(("sp", "tp"), None),
            P("sp", None),
            P(),
            P(),
            P("sp", "tp"),
            P("sp", "tp"),
            P("sp", "tp"),
            P(None, "tp"),
            P(None, "tp"),
            P(None, "tp"),
            P("tp", None),
            P("tp"),
            P("tp"),
            P(),
        ),
        out_specs=P(("sp", "tp"), None),
        check_vma=False,
    )
```

profile of v0, /device:TPU:1, one launch (start us, length us, event | category | flops | bytes accessed | tf_op | source)
XLA Modules:
  0.0 375.7 jit_solution(12642120670295756358)
XLA Ops:
  10.3 8.4 %all-to-all-start = ((f32[16,2,3,256]{3,1,2,0:T(2,128)}), f32[16,2,3,256]{3,1,2,0:T(2,128)S(1)}, u32[]{:S(2)}, u32[]{:S(2)}) async-start(f32[16,2,3,256]{3,1,2,0:T(2,128)} %broadcast_in_dim.10), calls=%async_computation | async-start | bytes 196608 | tf_op jit(solution)/shard_map/all_to_all | solution.py:12
  19.9 5.5 %all-to-all-done = f32[16,2,3,256]{3,1,2,0:T(2,128)S(1)} async-done(((f32[16,2,3,256]{3,1,2,0:T(2,128)}), f32[16,2,3,256]{3,1,2,0:T(2,128)S(1)}, u32[]{:S(2)}, u32[]{:S(2)}) %all-to-all-start) | async-done | bytes 98336 | tf_op jit(solution)/shard_map/all_to_all | solution.py:12
  26.1 6.5 %all-to-all-start.1 = ((f32[8,2,3,256]{3,1,2,0:T(2,128)}), f32[8,2,3,256]{3,1,2,0:T(2,128)S(1)}, u32[]{:S(2)}, u32[]{:S(2)}) async-start(f32[8,2,3,256]{3,1,2,0:T(2,128)} %broadcast_in_dim.11), calls=%async_computation.1 | async-start | bytes 98304 | tf_op jit(solution)/shard_map/all_to_all | solution.py:12
  32.6 4.8 %all-to-all-done.1 = f32[8,2,3,256]{3,1,2,0:T(2,128)S(1)} async-done(((f32[8,2,3,256]{3,1,2,0:T(2,128)}), f32[8,2,3,256]{3,1,2,0:T(2,128)S(1)}, u32[]{:S(2)}, u32[]{:S(2)}) %all-to-all-start.1) | async-done | bytes 49184 | tf_op jit(solution)/shard_map/all_to_all | solution.py:12
  38.0 2.0 fusion.74
  40.1 24.0 %all-gather.3.cloned.1.call-done = bf16[768,2048]{1,0:T(8,128)(2,1)} async-done(((bf16[96,2048]{1,0:T(8,128)(2,1)}), bf16[768,2048]{1,0:T(8,128)(2,1)}) %all-gather.3.cloned.1.call-update) | async-done | bytes 3145744 | tf_op jit(solution)/shard_map/all_gather | solution.py:129
  64.2 5.5 %fusion.52 = bf16[768,768]{0,1:T(8,128)(2,1)S(1)} fusion(bf16[768,2048]{1,0:T(8,128)(2,1)} %all-gather.3.cloned.1.call-done, bf16[2048,256]{1,0:T(8,128)(2,1)} %param.25, bf16[2048,256]{1,0:T(8,128)(2,1)} %param.24, bf16[2048,256]{1,0:T(8,128)(2,1)} %param.23), kind=kOutput, calls=%fused_computation.59 | convolution fusion | flops 2425946112 | bytes 7471104 | tf_op jit(solution)/shard_map/dot_general | solution.py:128
  72.5 30.3 %all_to_all.15 = bf16[16,64,512]{2,1,0:T(8,128)(2,1)S(1)} all-to-all(bf16[16,64,512]{2,1,0:T(8,128)(2,1)S(1)} %broadcast_in_dim.12), channel_id=1, replica_groups=mesh['sp'=16,'tp'=8] {'sp'}, dimensions={0} | all-to-all | bytes 2097152 | tf_op jit(solution)/shard_map/all_to_all | solution.py:12
  105.4 2.6 fusion.33
  108.1 3.5 fusion.37
  112.8 3.0 fusion.61
  115.9 3.1 fusion.64
  119.0 48.6 %all-gather.5.cloned.1.call-done = bf16[12288,512]{0,1:T(8,128)(2,1)} async-done(((bf16[768,512]{0,1:T(8,128)(2,1)}), bf16[12288,512]{0,1:T(8,128)(2,1)}) %all-gather.5.cloned.1.call-update) | async-done | bytes 12582928 | tf_op jit(solution)/shard_map/all_gather | solution.py:154
  167.6 16.6 %copy.48 = bf16[12288,512]{1,0:T(8,128)(2,1)} copy(bf16[12288,512]{0,1:T(8,128)(2,1)} %all-gather.5.cloned.1.call-done) | data formatting | bytes 25165824 | tf_op jit(solution)/shard_map/all_gather | solution.py:154
  184.3 145.0 %while.20 = (s32[]{:T(128)}, f32[2,768]{1,0:T(2,128)S(1)}, f32[2,768]{1,0:T(2,128)}, f32[768,2,128]{0,2,1:T(8,128)}, f32[2,768]{1,0:T(2,128)S(1)}, /*index=5*/f3...) while((s32[]{:T(128)}, f32[2,768]{1,0:T(2,128)S(1)}, ...), condition=%wide.region_12.13_spmd, body=%wide.region_7.12_spmd.sunk | while | flops 1243358208 | bytes 68322168 | solution.py:90
  193.1 2.6 fusion.136
  205.1 2.6 fusion.136
  217.2 2.6 fusion.136
  229.3 2.6 fusion.136
  241.4 2.6 fusion.136
  253.5 2.6 fusion.136
  260.4 1.8 bitcast_reduce_fusion.3
  265.6 2.6 fusion.136
  277.6 2.6 fusion.136
  284.5 1.8 bitcast_reduce_fusion.3
  289.7 2.6 fusion.136
  301.8 2.6 fusion.136
  313.9 2.6 fusion.136
  326.0 2.6 fusion.136
  331.7 2.7 convolution_convert_fusion
  334.4 32.9 %reduce-scatter.2.cloned.1.call-done = bf16[96,2048]{1,0:T(8,128)(2,1)} async-done(((bf16[768,2048]{1,0:T(8,128)(2,1)}), bf16[96,2048]{1,0:T(8,128)(2,1)}) %reduce-scatter.2.cloned.1.call-update) | async-done | bytes 393232 | tf_op jit(solution)/shard_map/reduce_scatter | solution.py:164
  367.3 1.9 fusion.75
  (396 shorter events, 123.1 us)
Async XLA Ops:
  6.5 325.2 %copy-start = (bf16[256,2048]{1,0:T(8,128)(2,1)S(1)}, bf16[256,2048]{1,0:T(8,128)(2,1)}, u32[]{:S(2)}) copy-start(bf16[256,2048]{1,0:T(8,128)(2,1)} %param.26) | copy-start | bytes 3145732
  10.3 15.1 %all-to-all-start = ((f32[16,2,3,256]{3,1,2,0:T(2,128)}), f32[16,2,3,256]{3,1,2,0:T(2,128)S(1)}, u32[]{:S(2)}, u32[]{:S(2)}) async-start(f32[16,2,3,256]{3,1,2,0:T(2,128)} %broadcast_in_dim.10), calls=%async_computation | async-start | bytes 196608 | tf_op jit(solution)/shard_map/all_to_all | solution.py:12
  26.1 11.3 %all-to-all-start.1 = ((f32[8,2,3,256]{3,1,2,0:T(2,128)}), f32[8,2,3,256]{3,1,2,0:T(2,128)S(1)}, u32[]{:S(2)}, u32[]{:S(2)}) async-start(f32[8,2,3,256]{3,1,2,0:T(2,128)} %broadcast_in_dim.11), calls=%async_computation.1 | async-start | bytes 98304 | tf_op jit(solution)/shard_map/all_to_all | solution.py:12
  32.6 31.5 %all-gather.3.cloned.1.call-start = ((), (), s32[]{:S(2)}) async-start(), calls=%async_computation.4 | async-start | bytes 3538944 | tf_op jit(solution)/shard_map/all_gather | solution.py:129
  40.0 31.7 %copy-start.11 = (bf16[64,2048]{1,0:T(8,128)(2,1)S(1)}, bf16[64,2048]{1,0:T(8,128)(2,1)}, u32[]{:S(2)}) copy-start(bf16[64,2048]{1,0:T(8,128)(2,1)} %param.17) | copy-start | bytes 786436
  40.0 31.8 %copy-start.13 = (f32[2048]{0:T(1024)S(1)}, f32[2048]{0:T(1024)}, u32[]{:S(2)}) copy-start(f32[2048]{0:T(1024)} %param.19) | copy-start | bytes 24580
  40.0 31.8 %copy-start.14 = (bf16[2048,256]{1,0:T(8,128)(2,1)S(1)}, bf16[2048,256]{1,0:T(8,128)(2,1)}, u32[]{:S(2)}) copy-start(bf16[2048,256]{1,0:T(8,128)(2,1)} %param.25) | copy-start | bytes 3145732
  40.1 31.8 %copy-start.15 = (bf16[2048,256]{1,0:T(8,128)(2,1)S(1)}, bf16[2048,256]{1,0:T(8,128)(2,1)}, u32[]{:S(2)}) copy-start(bf16[2048,256]{1,0:T(8,128)(2,1)} %param.24) | copy-start | bytes 3145732
  40.1 127.6 %all-gather.5.cloned.1.call-start = ((), (), s32[]{:S(2)}) async-start(), calls=%async_computation.5 | async-start | bytes 13369344 | tf_op jit(solution)/shard_map/all_gather | solution.py:154
  71.6 295.7 %reduce-scatter.2.cloned.1.call-start = ((), (), s32[]{:S(2)}) async-start(), calls=%async_computation.6 | async-start | bytes 3538944 | tf_op jit(solution)/shard_map/reduce_scatter | solution.py:164
  191.4 4.3 %copy-start.4 = (f32[768,2,128]{0,2,1:T(8,128)}, f32[768,2,128]{0,2,1:T(8,128)S(1)}, u32[]{:S(2)}) copy-start(f32[768,2,128]{0,2,1:T(8,128)S(1)} %fusion.138) | copy-start | bytes 2359300 | tf_op jit(solution)/shard_map/while
  203.4 4.3 %copy-start.4 = (f32[768,2,128]{0,2,1:T(8,128)}, f32[768,2,128]{0,2,1:T(8,128)S(1)}, u32[]{:S(2)}) copy-start(f32[768,2,128]{0,2,1:T(8,128)S(1)} %fusion.138) | copy-start | bytes 2359300 | tf_op jit(solution)/shard_map/while
  205.1 2.7 copy-start.6
  205.1 2.7 copy-start.7
  205.1 2.7 copy-start.9
  215.5 4.3 %copy-start.4 = (f32[768,2,128]{0,2,1:T(8,128)}, f32[768,2,128]{0,2,1:T(8,128)S(1)}, u32[]{:S(2)}) copy-start(f32[768,2,128]{0,2,1:T(8,128)S(1)} %fusion.138) | copy-start | bytes 2359300 | tf_op jit(solution)/shard_map/while
  227.6 4.3 %copy-start.4 = (f32[768,2,128]{0,2,1:T(8,128)}, f32[768,2,128]{0,2,1:T(8,128)S(1)}, u32[]{:S(2)}) copy-start(f32[768,2,128]{0,2,1:T(8,128)S(1)} %fusion.138) | copy-start | bytes 2359300 | tf_op jit(solution)/shard_map/while
  229.3 2.7 copy-start.6
  229.3 2.7 copy-start.7
  229.3 2.7 copy-start.9
  239.7 4.3 %copy-start.4 = (f32[768,2,128]{0,2,1:T(8,128)}, f32[768,2,128]{0,2,1:T(8,128)S(1)}, u32[]{:S(2)}) copy-start(f32[768,2,128]{0,2,1:T(8,128)S(1)} %fusion.138) | copy-start | bytes 2359300 | tf_op jit(solution)/shard_map/while
  251.8 4.3 %copy-start.4 = (f32[768,2,128]{0,2,1:T(8,128)}, f32[768,2,128]{0,2,1:T(8,128)S(1)}, u32[]{:S(2)}) copy-start(f32[768,2,128]{0,2,1:T(8,128)S(1)} %fusion.138) | copy-start | bytes 2359300 | tf_op jit(solution)/shard_map/while
  253.4 2.7 copy-start.6
  253.5 2.7 copy-start.7
  263.9 4.3 %copy-start.4 = (f32[768,2,128]{0,2,1:T(8,128)}, f32[768,2,128]{0,2,1:T(8,128)S(1)}, u32[]{:S(2)}) copy-start(f32[768,2,128]{0,2,1:T(8,128)S(1)} %fusion.138) | copy-start | bytes 2359300 | tf_op jit(solution)/shard_map/while
  275.9 4.3 %copy-start.4 = (f32[768,2,128]{0,2,1:T(8,128)}, f32[768,2,128]{0,2,1:T(8,128)S(1)}, u32[]{:S(2)}) copy-start(f32[768,2,128]{0,2,1:T(8,128)S(1)} %fusion.138) | copy-start | bytes 2359300 | tf_op jit(solution)/shard_map/while
  288.0 4.3 %copy-start.4 = (f32[768,2,128]{0,2,1:T(8,128)}, f32[768,2,128]{0,2,1:T(8,128)S(1)}, u32[]{:S(2)}) copy-start(f32[768,2,128]{0,2,1:T(8,128)S(1)} %fusion.138) | copy-start | bytes 2359300 | tf_op jit(solution)/shard_map/while
  300.1 4.3 %copy-start.4 = (f32[768,2,128]{0,2,1:T(8,128)}, f32[768,2,128]{0,2,1:T(8,128)S(1)}, u32[]{:S(2)}) copy-start(f32[768,2,128]{0,2,1:T(8,128)S(1)} %fusion.138) | copy-start | bytes 2359300 | tf_op jit(solution)/shard_map/while
  312.2 4.3 %copy-start.4 = (f32[768,2,128]{0,2,1:T(8,128)}, f32[768,2,128]{0,2,1:T(8,128)S(1)}, u32[]{:S(2)}) copy-start(f32[768,2,128]{0,2,1:T(8,128)S(1)} %fusion.138) | copy-start | bytes 2359300 | tf_op jit(solution)/shard_map/while
  324.3 4.3 %copy-start.4 = (f32[768,2,128]{0,2,1:T(8,128)}, f32[768,2,128]{0,2,1:T(8,128)S(1)}, u32[]{:S(2)}) copy-start(f32[768,2,128]{0,2,1:T(8,128)S(1)} %fusion.138) | copy-start | bytes 2359300 | tf_op jit(solution)/shard_map/while
  329.3 38.1 %copy-start.1 = (bf16[96,2048]{1,0:T(8,128)(2,1)S(1)}, bf16[96,2048]{1,0:T(8,128)(2,1)}, u32[]{:S(2)}) copy-start(bf16[96,2048]{1,0:T(8,128)(2,1)} %param.16) | copy-start | bytes 1179652
  329.3 38.1 %copy-start.12 = (f32[1,1,2048]{2,0,1:T(1,128)S(1)}, f32[1,1,2048]{2,0,1:T(1,128)}, u32[]{:S(2)}) copy-start(f32[1,1,2048]{2,0,1:T(1,128)} %get-tuple-element.135) | copy-start | bytes 24580
  (77 other events, 132.3 us)
Sparse Core Ops, SparseCore 0:
  40.1 23.9 all-gather.2
  71.8 95.8 all-gather.4
  334.6 32.7 reduce-scatter.1
where the time goes:
time: 380 us; the launch traced here: 376 us
  waiting for transfers between devices  116 us (31%)
  matrix products  94.3 us (25%)
  other arithmetic  52.9 us (14%)
  local copies, waits for them, and re-layouts  51.6 us (14%)
  blocking collectives  30.3 us (8%)
  starting transfers between devices  15 us (4%)
  between operations  13.3 us (4%)
    all_gather x1, waiting for transfers between devices, per_device(): portion = lax.all_gather(latent_kv, 'sp', axis=0, tiled=True)  48.6 us
    dot_general x26, matrix products, absorb(): jnp.einsum('hqk,khd->qhd', raised.astype(jnp.bfloat16), value_rows, prefe...  45.1 us
    dot_general x26, matrix products, absorb(): jnp.einsum('qhd,khd->hqk', queries[:, :, which_map], key_rows[:, :, which...  37.5 us
    reduce_sum x13, other arithmetic, absorb(): weight = weight * faded + jnp.sum(raised, axis=2)  34.8 us
    reduce_scatter x1, waiting for transfers between devices, per_device(): lax.psum_scatter(jnp.dot(flattened, w_out, preferred_element_type=jnp.flo...  32.9 us
    all_to_all x1, blocking collectives, copy_for_each(): lax.all_to_all(jnp.broadcast_to(shard[None], (count, *shard.shape)), axis...  30.3 us
    all_gather x1, waiting for transfers between devices, per_device(): lax.all_gather(own_rows, 'tp', axis=0, tiled=True)  24 us
    dynamic_slice x24, local copies, waits for them, and re-layouts, absorb_rows(): running, unused = lax.scan(advance, running, (stacked, flag_blocks))  21.9 us
  transfers between devices with their start and end apart: 5, of which 5 were waited for; matrix products, arithmetic and copies ran while one was open for 5% of the time, Pallas kernels for 0%

commit v1 on v0

v1 whole, which is shorter than its diff:
```python
import functools
import math

import jax
import jax.numpy as jnp
from jax import lax
from jax.experimental import pallas as pl
from jax.experimental.pallas import tpu as pltpu
from jax.sharding import PartitionSpec as P

EPS = 1e-06
MESH = pl.DeviceIdType.MESH
BF = jnp.bfloat16
F32 = jnp.float32
LOG2E = math.log2(math.e)
SCALE = LOG2E / 8.0
ROWS = 96
PAIR = 192
OWN = 768
CTXR = 64
BLOCK = 2 * OWN + 2 * CTXR
QT = 512
NQ = 3
UNITS = 6
AHEAD = 2


def gray(n):
    return n + n // 2 - 2 * ((n // 2) * (n % 2))


def remote(src, dst, send, recv, sp, tp):
    return pltpu.make_async_remote_copy(
        src_ref=src, dst_ref=dst, send_sem=send, recv_sem=recv, device_id=(sp, tp), device_id_type=MESH
    )


def round_y(own, buf, rows, send, recv, s, y, c):
    up, down = ((y + 1) % 4) * 2 + c, ((y + 3) % 4) * 2 + c
    sib = y * 2 + 1 - c
    half = rows // 2

    def at(slot, offset, size):
        return buf.at[slot, pl.ds(pl.multiple_of(c * rows + offset, 16), size)]

    return [
        remote(own, at(0, 0, rows), send.at[0], recv.at[0], s, sib),
        remote(own, at(1, 0, rows), send.at[1], recv.at[1], s, up),
        remote(own, at(2, 0, rows), send.at[2], recv.at[2], s, down),
        remote(at(1, 0, half), at(3, 0, half), send.at[3], recv.at[3], s, up),
        remote(at(2, half, half), at(3, half, half), send.at[4], recv.at[4], s, down),
        remote(at(1, 0, rows), at(1, 0, rows), send.at[5], recv.at[5], s, sib),
        remote(at(2, 0, rows), at(2, 0, rows), send.at[6], recv.at[6], s, sib),
        remote(at(3, 0, rows), at(3, 0, rows), send.at[7], recv.at[7], s, sib),
    ]


def kernel(
    latent, context, cond, gain, mod_shift, mod_scale, mod_gate, w_query, w_key, w_value, w_out, lambdas,
    context_bias, head_gain, out,
    lat, part, msg, msg2, mods, qv, kvown, qown, kv, qb, qm, vctx, sscr, acc, peak, nsend, nrm, wall,
    lsend, lrecv, wsend, wrecv, msend, mrecv, nsd, nrc, zsend, zqsend, kvrecv, qrecv, fsib, fplus, fminus,
    osend, orecv, local,
):
    s, t = lax.axis_index("sp"), lax.axis_index("tp")
    z, x, y, c = s // 4, s % 4, t // 2, t % 2
    sib = y * 2 + 1 - c

    barrier = pltpu.get_barrier_semaphore()
    for d in range(1, 16):
        pl.semaphore_signal(barrier, inc=1, device_id=((s + d) % 16, t), device_id_type=MESH)
    for d in range(1, 8):
        pl.semaphore_signal(barrier, inc=1, device_id=(s, (t + d) % 8), device_id_type=MESH)
    pl.semaphore_wait(barrier, 22)

    lcp = round_y(latent, lat, ROWS, lsend, lrecv, s, y, c)
    for k in (1, 2, 0):
        lcp[k].start()
    lat[0, pl.ds(pl.multiple_of(c * ROWS, 16), ROWS), :] = latent[...]

    cols = cond[:, pl.ds(pl.multiple_of(s * 128, 128), 128)]
    activated = (cols / (1.0 + jnp.exp(-cols))).astype(BF)
    activated = jnp.concatenate([activated.astype(F32), jnp.zeros((6, 128), F32)], axis=0).astype(BF)
    for index, matrix in enumerate((mod_shift, mod_scale, mod_gate)):
        product = jnp.dot(activated, matrix[...], preferred_element_type=F32)
        for r in range(2):
            for half in range(2):
                row = index * 4 + r * 2 + half
                msg[row : row + 1, :] = product[r : r + 1, half * 128 : half * 128 + 128]
    msg[12:16, :] = jnp.zeros((4, 128), F32)
    mcp = []
    for d in range(1, 16):
        mcp.append(remote(msg, part.at[s], msend.at[d], mrecv.at[d], (s + d) % 16, t))
        mcp[-1].start()
    part[s] = msg[...]
    for copy in mcp:
        copy.wait_recv()
    total = part[0]
    for k in range(1, 16):
        total = total + part[k]
    msg2[...] = total
    msg2[12:13, 0:2] = lambdas[...]
    msg2[13:14, 0:2] = context_bias[...]
    ncp = []
    for d in range(1, 8):
        ncp.append(remote(msg2, mods.at[t], nsd.at[d], nrc.at[d], s, (t + d) % 8))
        ncp[-1].start()
    mods[t] = msg2[...]
    for copy in ncp:
        copy.wait_recv()

    def vector(index, r):
        row = index * 4 + r * 2
        return jnp.concatenate([mods[k, row + h : row + h + 1, :] for k in range(8) for h in range(2)], axis=1)

    def modulate(rows, r):
        rows = rows.astype(F32)
        normal = rows * lax.rsqrt(jnp.mean(rows * rows, axis=1, keepdims=True) + EPS)
        return (normal * gain[...] * (1.0 + vector(1, r)) + vector(0, r)).astype(BF)

    hidden = modulate(context[...], 1)
    keys = jnp.dot(hidden, w_key[...], preferred_element_type=F32).astype(BF)
    values = jnp.dot(hidden, w_value[...], preferred_element_type=F32).astype(BF)
    for i in range(2):
        kvown[i, 2 * OWN : 2 * OWN + CTXR, :] = keys[:, 128 * i : 128 * i + 128]
        kvown[i, 2 * OWN + CTXR : BLOCK, :] = values[:, 128 * i : 128 * i + 128]

    def project(p):
        hidden = modulate(lat[p], 0)
        rows = slice(PAIR * p, PAIR * p + PAIR)
        qv[0, rows, :] = jnp.dot(hidden, w_query[...], preferred_element_type=F32)
        keys = jnp.dot(hidden, w_key[...], preferred_element_type=F32).astype(BF)
        for i in range(2):
            kvown[i, rows, :] = keys[:, 128 * i : 128 * i + 128]
        qv[1, rows, :] = jnp.dot(hidden, w_value[...], preferred_element_type=F32)

    lcp[0].wait_recv()
    project(0)
    lcp[1].wait_recv()
    lcp[3].start()
    lcp[5].start()
    lcp[2].wait_recv()
    lcp[4].start()
    lcp[6].start()
    wcp = round_y(w_out, wall, 256, wsend, wrecv, s, y, c)
    for k in (1, 2, 0):
        wcp[k].start()
    wall[0, pl.ds(pl.multiple_of(c * 256, 256), 256), :] = w_out[...]
    lcp[5].wait_recv()
    project(1)
    lcp[6].wait_recv()
    project(2)
    lcp[3].wait_recv()
    lcp[4].wait_recv()
    lcp[7].start()
    lcp[7].wait_recv()
    project(3)
    for a in range(6):
        for i in range(2):
            rows, columns = slice(128 * a, 128 * a + 128), slice(128 * i, 128 * i + 128)
            kvown[i, OWN + 128 * a : OWN + 128 * a + 128, :] = qv[1, rows, columns].T.astype(BF)
            qown[a // 3, i, a % 3] = qv[0, rows, columns].T.astype(BF)

    for i in range(2):
        j = 2 * c + i
        dest = j * 4 + x

        def q_here():
            return pltpu.make_async_copy(qown.at[0, i], qb.at[z], qrecv.at[z])

        def kv_here():
            return pltpu.make_async_copy(kvown.at[i], kv.at[s], kvrecv.at[s])

        remote(qown.at[1, i], qb.at[z], zqsend.at[i, 1], qrecv.at[z], dest, sib).start()

        @pl.when(j == z)
        def _():
            q_here().start()
            kv_here().start()

        @pl.when(j != z)
        def _():
            remote(qown.at[0, i], qb.at[z], zqsend.at[i, 0], qrecv.at[z], dest, t).start()
            remote(kvown.at[i], kv.at[s], zsend.at[i], kvrecv.at[s], dest, t).start()

    primary = c == z // 2
    plus, minus = z * 4 + (x + 1) % 4, z * 4 + (x + 3) % 4

    def to_sib(b):
        return remote(kv.at[b], kv.at[b], fsib.at[b], kvrecv.at[b], s, sib)

    def to_plus(b):
        return remote(kv.at[b], kv.at[b], fplus.at[b], kvrecv.at[b], plus, t)

    def to_minus(b):
        return remote(kv.at[b], kv.at[b], fminus.at[b], kvrecv.at[b], minus, t)

    def place(n):
        dz, dx = gray(n % 4), gray(n // 4)
        return dz, dx, ((z + dz) % 4) * 4 + (x + dx) % 4

    def goes_plus(dz, dx):
        return (dx == 0) | ((dx == 3) & (dz < 2))

    def goes_minus(dz, dx):
        return (dx == 0) | ((dx == 1) & (dz >= 2))

    def take(n):
        dz, dx, b = place(n)
        pltpu.make_async_copy(kvown.at[0], kv.at[b], kvrecv.at[b]).wait()

        @pl.when(primary)
        def _():
            @pl.when(goes_plus(dz, dx))
            def _():
                to_plus(b).start()

            @pl.when(goes_minus(dz, dx))
            def _():
                to_minus(b).start()

            to_sib(b).start()

        return b

    for k in range(4):
        pltpu.make_async_copy(qown.at[0, 0], qb.at[k], qrecv.at[k]).wait()
    for tile in range(NQ):
        for r in range(4):
            chunk = 4 * tile + r
            columns = slice(128 * r, 128 * r + 128)
            block = qb[chunk // 3, chunk % 3]
            zero = jnp.zeros((64, 128), BF)
            qm[0, tile, 0:64, columns] = block[0:64]
            qm[0, tile, 64:128, columns] = zero
            qm[1, tile, 0:64, columns] = zero
            qm[1, tile, 64:128, columns] = block[64:128]
    for u in range(UNITS):
        acc[u] = jnp.zeros_like(acc[u])
        peak[u] = jnp.full_like(peak[u], -1e30)

    units = [(m, tile) for tile in range(NQ) for m in range(2)]

    def absorb(keys, lhs, size, bias):
        tops = {}

        def score(u):
            m, tile = units[u]
            raw = jnp.dot(keys, qm[m, tile], preferred_element_type=F32)
            sscr[u % (AHEAD + 1), 0:size, :] = raw
            tops[u] = jnp.max(raw, axis=0, keepdims=True) * SCALE

        for u in range(AHEAD):
            score(u)
        for u in range(UNITS):
            if u + AHEAD < UNITS:
                score(u + AHEAD)
            top = tops[u] if bias is None else tops[u] + bias
            old = peak[u]
            new = jnp.maximum(old, top)
            peak[u] = new
            faded = jnp.exp2(old - new)
            shift = new if bias is None else new - bias
            probs = jnp.exp2(sscr[u % (AHEAD + 1), 0:size, :] * SCALE - shift).astype(BF)
            acc[u] = acc[u] * faded + jnp.dot(lhs, probs, preferred_element_type=F32)

    def latent_step(n, carry):
        b = take(n)

        @pl.when(n == 4)
        def _():
            wcp[1].wait_recv()
            wcp[3].start()
            wcp[5].start()
            wcp[2].wait_recv()
            wcp[4].start()
            wcp[6].start()

        @pl.when(n == 12)
        def _():
            wcp[3].wait_recv()
            wcp[4].wait_recv()
            wcp[7].start()

        keys = kv[b, 0:OWN, :]
        lhs = jnp.concatenate([kv[b, OWN + 128 * a : OWN + 128 * a + 128, :] for a in range(6)], axis=1)
        lhs = jnp.concatenate([lhs, jnp.ones((16, OWN), BF)], axis=0)
        absorb(keys, lhs, OWN, None)
        return carry

    lax.fori_loop(0, 16, latent_step, 0)

    lane = lax.broadcasted_iota(jnp.int32, (1, 128), 1)
    owner = y * 2 + z // 2

    def pick(row):
        return jnp.sum(jnp.where(lane == z % 2, mods[owner, row : row + 1, :], 0.0), axis=1, keepdims=True)

    for k in range(8):
        pair = jnp.concatenate([kv[2 * k, 2 * OWN + CTXR : BLOCK, :], kv[2 * k + 1, 2 * OWN + CTXR : BLOCK, :]], axis=0)
        vctx[:, 128 * k : 128 * k + 128] = pair.astype(F32).T.astype(BF)
    keys = jnp.concatenate([kv[k, 2 * OWN : 2 * OWN + CTXR, :] for k in range(16)], axis=0)
    lhs = jnp.concatenate([vctx[...], jnp.ones((16, 16 * CTXR), BF)], axis=0)
    absorb(keys, lhs, 16 * CTXR, pick(13) * LOG2E)

    lam = pick(12)
    for tile in range(NQ):
        one, two = acc[2 * tile], acc[2 * tile + 1]
        mixed = one[0:128] / one[128:129] - lam * (two[0:128] / two[128:129])
        normed = mixed * lax.rsqrt(jnp.mean(mixed * mixed, axis=0, keepdims=True) + EPS)
        for r in range(4):
            block = normed[:, 128 * r : 128 * r + 128].T * head_gain[...]
            row = QT * tile + 128 * r
            nsend[row : row + 128, :] = block.astype(BF)

    head = y * 4 + z
    half = 1 - (c == z // 2).astype(jnp.int32)
    ocp = []
    for k in range(4):
        for e in range(4):
            offset = half if e // 2 == 0 else 3 * half + 3
            target = ((y + offset) % 4) * 2 + e % 2
            src = nsend.at[pl.ds(pl.multiple_of(384 * k + ROWS * e, 16), ROWS)]
            here = (k == z) & (target == t)
            ocp.append((src, k * 4 + x, target, here, 4 * k + e))
    for src, sp, tp, here, index in ocp:

        @pl.when(here)
        def _():
            pltpu.make_async_copy(src, nrm.at[head], orecv.at[head]).start()

        @pl.when(jnp.logical_not(here))
        def _():
            remote(src, nrm.at[head], osend.at[index], orecv.at[head], sp, tp).start()

    for k in (0, 5, 6, 7):
        wcp[k].wait_recv()
    for k in range(16):
        pltpu.make_async_copy(nsend.at[0:ROWS], nrm.at[k], orecv.at[k]).wait()

    attended = jnp.zeros((ROWS, 2048), F32)
    for p in range(4):
        group = ((y + (0, 3, 1, 2)[p]) % 4) * 2
        for k in range(2):
            rows = jnp.concatenate([nrm[2 * (group + k)], nrm[2 * (group + k) + 1]], axis=1)
            product = jnp.dot(rows, wall[p, 256 * k : 256 * k + 256, :], preferred_element_type=F32)
            attended = attended + product.astype(BF).astype(F32)
    gate = vector(2, 0)
    out[...] = (latent[...].astype(F32) + gate * attended.astype(BF).astype(F32)).astype(BF)

    for copy in lcp + wcp + mcp + ncp:
        copy.wait_send()
    for i in range(2):
        j = 2 * c + i
        remote(qown.at[1, i], qb.at[z], zqsend.at[i, 1], qrecv.at[z], j * 4 + x, sib).wait_send()

        @pl.when(j != z)
        def _():
            remote(qown.at[0, i], qb.at[z], zqsend.at[i, 0], qrecv.at[z], j * 4 + x, t).wait_send()
            remote(kvown.at[i], kv.at[s], zsend.at[i], kvrecv.at[s], j * 4 + x, t).wait_send()

    @pl.when(primary)
    def _():
        def sent(n, carry):
            dz, dx, b = place(n)

            @pl.when(goes_plus(dz, dx))
            def _():
                to_plus(b).wait_send()

            @pl.when(goes_minus(dz, dx))
            def _():
                to_minus(b).wait_send()

            to_sib(b).wait_send()
            return carry

        lax.fori_loop(0, 16, sent, 0)

    for src, sp, tp, here, index in ocp:

        @pl.when(jnp.logical_not(here))
        def _():
            remote(src, nrm.at[head], osend.at[index], orecv.at[head], sp, tp).wait_send()


def per_device(
    latent, context, conditioning, norm_gain, mod_shift, mod_scale, mod_gate, w_query, w_key, w_value, w_out,
    lambdas, context_bias, head_gain,
):
    dma = pltpu.SemaphoreType.DMA
    vmem = pl.BlockSpec(memory_space=pltpu.VMEM)
    return pl.pallas_call(
        kernel,
        name="block",
        out_shape=jax.ShapeDtypeStruct(latent.shape, BF),
        in_specs=[vmem] * 14,
        out_specs=vmem,
        scratch_shapes=[
            pltpu.VMEM((4, PAIR, 2048), BF),
            pltpu.VMEM((16, 16, 128), F32),
            pltpu.VMEM((16, 128), F32),
            pltpu.VMEM((16, 128), F32),
            pltpu.VMEM((8, 16, 128), F32),
            pltpu.VMEM((2, OWN, 256), F32),
            pltpu.VMEM((2, BLOCK, 128), BF),
            pltpu.VMEM((2, 2, 3, 128, 128), BF),
            pltpu.VMEM((16, BLOCK, 128), BF),
            pltpu.VMEM((4, 3, 128, 128), BF),
            pltpu.VMEM((2, NQ, 128, QT), BF),
            pltpu.VMEM((128, 16 * CTXR), BF),
            pltpu.VMEM((AHEAD + 1, 16 * CTXR, QT), F32),
            pltpu.VMEM((UNITS, 144, QT), F32),
            pltpu.VMEM((UNITS, 1, QT), F32),
            pltpu.VMEM((1536, 128), BF),
            pltpu.VMEM((16, ROWS, 128), BF),
            pltpu.VMEM((4, 512, 2048), BF),
            dma((8,)), dma((8,)), dma((8,)), dma((8,)),
            dma((16,)), dma((16,)), dma((8,)), dma((8,)),
            dma((2,)), dma((2, 2)), dma((16,)), dma((4,)),
            dma((16,)), dma((16,)), dma((16,)),
            dma((16,)), dma((16,)), dma((1,)),
        ],
        compiler_params=pltpu.CompilerParams(
            collective_id=0, has_side_effects=True, vmem_limit_bytes=60 * 2**20
        ),
    )(
        latent, context, conditioning, norm_gain.reshape(1, -1), mod_shift, mod_scale, mod_gate, w_query, w_key,
        w_value, w_out, lambdas.reshape(1, -1), context_bias.reshape(1, -1), head_gain.reshape(1, -1),
    )


def solution(mesh):
    return jax.shard_map(
        per_device,
        mesh=mesh,
        in_specs=(
            P(("sp", "tp"), None),
            P("sp", None),
            P(),
            P(),
            P("sp", "tp"),
            P("sp", "tp"),
            P("sp", "tp"),
            P(None, "tp"),
            P(None, "tp"),
            P(None, "tp"),
            P("tp", None),
            P("tp"),
            P("tp"),
            P(),
        ),
        out_specs=P(("sp", "tp"), None),
        check_vma=False,
    )
```

time: 380 us -> 110 us (0.29); the launches traced: 376 us -> 110 us
  waiting for transfers between devices: 116 us -> 0 us
  Pallas kernels: 0 us -> 108 us
  matrix products: 94.3 us -> 0 us
  other arithmetic: 52.9 us -> 0 us
  local copies, waits for them, and re-layouts: 51.6 us -> 1.77 us
  blocking collectives: 30.3 us -> 0 us
  starting transfers between devices: 15 us -> 0 us
  between operations: 13.3 us -> 0.01 us
    pallas_call x0 -> x1, Pallas kernels: none -> 108 us  [per_device(): pl.pallas_call(kernel, name='block', out_shape=jax.ShapeDtypeStruct(laten...]
    dot_general x58 -> x0, matrix products: 94.3 us -> none  [the longest x26 45.1 us: absorb(): jnp.einsum('hqk,khd->qhd', raised.astype(jnp.bfloat16), value_rows, prefe...]
    all_gather x2 -> x0, waiting for transfers between devices: 72.7 us -> none  [the longest x1 48.6 us: per_device(): portion = lax.all_gather(latent_kv, 'sp', axis=0, tiled=True)]
    reduce_sum x17 -> x0, other arithmetic: 37.9 us -> none  [the longest x13 34.8 us: absorb(): weight = weight * faded + jnp.sum(raised, axis=2)]
    reduce_scatter x1 -> x0, waiting for transfers between devices: 32.9 us -> none  [per_device(): lax.psum_scatter(jnp.dot(flattened, w_out, preferred_element_type=jnp.flo...]
    all_to_all x1 -> x0, blocking collectives: 30.3 us -> none  [copy_for_each(): lax.all_to_all(jnp.broadcast_to(shard[None], (count, *shard.shape)), axis...]
    dynamic_slice x24 -> x0, local copies, waits for them, and re-layouts: 21.9 us -> none  [absorb_rows(): running, unused = lax.scan(advance, running, (stacked, flag_blocks))]
    all_gather x1 -> x0, local copies, waits for them, and re-layouts: 16.6 us -> none  [per_device(): portion = lax.all_gather(latent_kv, 'sp', axis=0, tiled=True)]
  transfers between devices with their start and end apart: 5 -> 0, of which waited for: 5 -> 0; matrix products, arithmetic and copies ran while one was open for 5% -> 0% of each run, Pallas kernels for 0% -> 0%
where the time goes in v1:
time: 110 us
  Pallas kernels  108 us (98%)
  local copies, waits for them, and re-layouts  1.77 us (2%)
    pallas_call x1, Pallas kernels, per_device(): pl.pallas_call(kernel, name='block', out_shape=jax.ShapeDtypeStruct(laten...  108 us

profile of v1, /device:TPU:1, one launch (start us, length us, event | category | flops | bytes accessed | tf_op | source)
XLA Modules:
  0.0 109.7 jit_solution(15583289228809269262)
XLA Ops:
  0.0 107.9 %block.1 = bf16[96,2048]{1,0:T(8,128)(2,1)} custom-call(bf16[96,2048]{1,0:T(8,128)(2,1)} %latent.1, bf16[64,2048]{1,0:T(8,128)(2,1)} %context.1, f32[2,2048]{1,0:T(2,128)} %cond.1, f32[1,2048]{1,0:T(1,128)} %bitcast.4, bf16[128,256]{1,0:T(8,128)(2,1)} %mod_shift.1, bf16[128,256]{1,0:T(8,128)(2,1)} %mod_scale.1, bf16[128,256]{1,0:T(8,128)(2,1)} %mod_gate.1, ...), custom_call_target="tpu_custom_call" | custom-call | tf_op jit(solution)/shard_map/block/pallas_call | solution.py:393
  107.9 1.8 %copy.16 = bf16[96,2048]{1,0:T(8,128)(2,1)} copy(bf16[96,2048]{1,0:T(8,128)(2,1)} %block.1) | data formatting | bytes 786432

commit v2 on v1

v2 whole, which is shorter than its diff:
```python
import functools
import math

import jax
import jax.numpy as jnp
from jax import lax
from jax.experimental import pallas as pl
from jax.experimental.pallas import tpu as pltpu
from jax.sharding import PartitionSpec as P

EPS = 1e-06
MESH = pl.DeviceIdType.MESH
BF = jnp.bfloat16
F32 = jnp.float32
LOG2E = math.log2(math.e)
SCALE = LOG2E / 8.0
ROWS = 96
PAIR = 192
OWN = 768
CTXR = 64
BLOCK = 2 * OWN + 2 * CTXR
QT = 256
NQ = 6
UNITS = 12
AHEAD = 3
ORDER = (
    (0, 0), (1, 0), (3, 0), (0, 1), (0, 3), (1, 1), (1, 3), (3, 1), (2, 0), (3, 3), (0, 2), (2, 1), (1, 2), (3, 2),
    (2, 3), (2, 2),
)
PASS = {
    1: ((3, 0),), 2: ((0, 1), (0, 3)), 4: ((1, 1), (1, 3)), 5: ((2, 0),), 6: ((3, 1), (3, 3)), 8: ((0, 2),),
    9: ((2, 1),), 10: ((1, 2), (3, 2)), 12: ((2, 3), (2, 2)),
}


def remote(src, dst, send, recv, sp, tp):
    return pltpu.make_async_remote_copy(
        src_ref=src, dst_ref=dst, send_sem=send, recv_sem=recv, device_id=(sp, tp), device_id_type=MESH
    )


def round_y(buf, rows, send, recv, s, y, c):
    up, down = ((y + 1) % 4) * 2 + c, ((y + 3) % 4) * 2 + c
    sib = y * 2 + 1 - c
    half = rows // 2

    def at(slot, offset, size):
        return buf.at[slot, pl.ds(pl.multiple_of(c * rows + offset, 16), size)]

    def one(k, source, slot, offset, size, to):
        return remote(at(source, offset, size), at(slot, offset, size), send.at[k], recv.at[k], s, to)

    return [
        one(0, 0, 0, 0, rows, sib),
        one(1, 0, 1, 0, half, up),
        one(2, 0, 2, half, half, down),
        one(3, 0, 1, half, half, up),
        one(4, 0, 2, 0, half, down),
        one(5, 1, 3, 0, half, up),
        one(6, 2, 3, half, half, down),
        one(7, 1, 1, 0, rows, sib),
        one(8, 2, 2, 0, rows, sib),
        one(9, 3, 3, 0, rows, sib),
    ]


def kernel(
    latent, context, cond, gain, mod_shift, mod_scale, mod_gate, w_query, w_key, w_value, w_out, lambdas,
    context_bias, head_gain, out,
    lat, ctx, mod, wqkv, part, msg, msg2, mods, qv, kvown, qown, kv, qb, qm, vctx, sscr, tops, acc, peak, nsend, nrm,
    wall, lsend, lrecv, wsend, wrecv, msend, mrecv, nsd, nrc, zsend, zqsend, kvrecv, qrecv, fsib, fplus, fminus,
    osend, orecv, local,
):
    s, t = lax.axis_index("sp"), lax.axis_index("tp")
    z, x, y, c = s // 4, s % 4, t // 2, t % 2
    sib = y * 2 + 1 - c

    barrier = pltpu.get_barrier_semaphore()
    for d in range(1, 8):
        pl.semaphore_signal(barrier, inc=1, device_id=(s, (t + d) % 8), device_id_type=MESH)
    for d in range(1, 16):
        pl.semaphore_signal(barrier, inc=1, device_id=((s + d) % 16, t), device_id_type=MESH)
    loads = [
        pltpu.make_async_copy(src, dst, local.at[k])
        for k, (src, dst) in enumerate(
            (
                (mod_shift, mod.at[0]),
                (mod_scale, mod.at[1]),
                (mod_gate, mod.at[2]),
                (latent, lat.at[0, pl.ds(pl.multiple_of(c * ROWS, 16), ROWS)]),
                (context, ctx),
                (w_query, wqkv.at[0]),
                (w_key, wqkv.at[1]),
                (w_value, wqkv.at[2]),
                (w_out, wall.at[0, pl.ds(pl.multiple_of(c * 256, 256), 256)]),
            )
        )
    ]
    for copy in loads:
        copy.start()

    cols = cond[:, pl.ds(pl.multiple_of(s * 128, 128), 128)]
    activated = (cols / (1.0 + jnp.exp(-cols))).astype(BF)
    activated = jnp.concatenate([activated.astype(F32), jnp.zeros((6, 128), F32)], axis=0).astype(BF)
    msg[12:16, :] = jnp.zeros((4, 128), F32)
    for index in range(3):
        loads[index].wait()
        product = jnp.dot(activated, mod[index], preferred_element_type=F32)
        for r in range(2):
            for half in range(2):
                row = index * 4 + r * 2 + half
                msg[row : row + 1, :] = product[r : r + 1, half * 128 : half * 128 + 128]
    loads[3].wait()
    pl.semaphore_wait(barrier, 22)

    mcp = [remote(msg, part.at[s], msend.at[d], mrecv.at[d], (s + d) % 16, t) for d in range(1, 16)]
    for copy in mcp:
        copy.start()
    lcp = round_y(lat, ROWS, lsend, lrecv, s, y, c)
    for k in (1, 2, 0):
        lcp[k].start()
    part[s] = msg[...]
    for copy in mcp:
        copy.wait_recv()
    total = part[0]
    for k in range(1, 16):
        total = total + part[k]
    msg2[...] = total
    msg2[12:13, 0:2] = lambdas[...]
    msg2[13:14, 0:2] = context_bias[...]
    ncp = [remote(msg2, mods.at[t], nsd.at[d], nrc.at[d], s, (t + d) % 8) for d in range(1, 8)]
    for copy in ncp:
        copy.start()
    lcp[3].start()
    lcp[4].start()
    mods[t] = msg2[...]
    lcp[1].wait_recv()
    lcp[5].start()
    lcp[2].wait_recv()
    lcp[6].start()
    for copy in ncp:
        copy.wait_recv()

    def vector(index, r):
        row = index * 4 + r * 2
        return jnp.concatenate([mods[k, row + h : row + h + 1, :] for k in range(8) for h in range(2)], axis=1)

    def modulate(rows, r):
        rows = rows.astype(F32)
        normal = rows * lax.rsqrt(jnp.mean(rows * rows, axis=1, keepdims=True) + EPS)
        return (normal * (gain[...] * (1.0 + vector(1, r))) + vector(0, r)).astype(BF)

    def project(p):
        hidden = modulate(lat[p], 0)
        rows = slice(PAIR * p, PAIR * p + PAIR)
        qv[0, rows, :] = jnp.dot(hidden, wqkv[0], preferred_element_type=F32)
        keys = jnp.dot(hidden, wqkv[1], preferred_element_type=F32).astype(BF)
        for i in range(2):
            kvown[i, rows, :] = keys[:, 128 * i : 128 * i + 128]
        qv[1, rows, :] = jnp.dot(hidden, wqkv[2], preferred_element_type=F32)

    for copy in loads[4:]:
        copy.wait()
    hidden = modulate(ctx[...], 1)
    keys = jnp.dot(hidden, wqkv[1], preferred_element_type=F32).astype(BF)
    values = jnp.dot(hidden, wqkv[2], preferred_element_type=F32).astype(BF)
    for i in range(2):
        kvown[i, 2 * OWN : 2 * OWN + CTXR, :] = keys[:, 128 * i : 128 * i + 128]
        kvown[i, 2 * OWN + CTXR : BLOCK, :] = values[:, 128 * i : 128 * i + 128]
    lcp[0].wait_recv()
    project(0)
    lcp[3].wait_recv()
    lcp[7].start()
    lcp[4].wait_recv()
    lcp[8].start()
    wcp = round_y(wall, 256, wsend, wrecv, s, y, c)
    for k in (1, 2, 3, 4, 0):
        wcp[k].start()
    lcp[7].wait_recv()
    project(1)
    lcp[8].wait_recv()
    project(2)
    lcp[5].wait_recv()
    lcp[6].wait_recv()
    lcp[9].start()
    lcp[9].wait_recv()
    project(3)
    for a in range(6):
        for i in range(2):
            rows, columns = slice(128 * a, 128 * a + 128), slice(128 * i, 128 * i + 128)
            qown[a // 3, i, a % 3] = qv[0, rows, columns].T.astype(BF)
    for a in range(6):
        for i in range(2):
            rows, columns = slice(128 * a, 128 * a + 128), slice(128 * i, 128 * i + 128)
            kvown[i, OWN + 128 * a : OWN + 128 * a + 128, :] = qv[1, rows, columns].T.astype(BF)

    primary = c == z // 2
    plus, minus = z * 4 + (x + 1) % 4, z * 4 + (x + 3) % 4

    def q_sib(i):
        return remote(qown.at[1, i], qb.at[z], zqsend.at[i, 1], qrecv.at[z], (2 * c + i) * 4 + x, sib)

    def q_own(i):
        return remote(qown.at[0, i], qb.at[z], zqsend.at[i, 0], qrecv.at[z], (2 * c + i) * 4 + x, t)

    def kv_own(i):
        return remote(kvown.at[i], kv.at[s], zsend.at[i], kvrecv.at[s], (2 * c + i) * 4 + x, t)

    def distance(i):
        return (2 * c + i - z + 4) % 4

    for i in range(2):
        q_sib(i).start()

        @pl.when(distance(i) != 0)
        def _():
            q_own(i).start()

        @pl.when(distance(i) == 0)
        def _():
            pltpu.make_async_copy(qown.at[0, i], qb.at[z], qrecv.at[z]).start()
            pltpu.make_async_copy(kvown.at[i], kv.at[s], kvrecv.at[s]).start()

    def source(dz, dx):
        return ((z + dz) % 4) * 4 + (x + dx) % 4

    def onward(dz, dx):
        b = source(dz, dx)
        block = kvown.at[z % 2] if (dz, dx) == (0, 0) else kv.at[b]
        copies = []
        if dx == 0 or (dx == 3 and dz < 2):
            copies.append(remote(block, kv.at[b], fplus.at[b], kvrecv.at[b], plus, t))
        if dx == 0 or (dx == 1 and dz >= 2):
            copies.append(remote(block, kv.at[b], fminus.at[b], kvrecv.at[b], minus, t))
        copies.append(remote(block, kv.at[b], fsib.at[b], kvrecv.at[b], s, sib))
        return copies

    def arrive(b):
        pltpu.make_async_copy(kvown.at[0], kv.at[b], kvrecv.at[b]).wait()

    def pass_on(dz, dx):
        arrive(source(dz, dx))
        for copy in onward(dz, dx):
            copy.start()

    @pl.when(primary)
    def _():
        for copy in onward(0, 0):
            copy.start()

    for i in range(2):

        @pl.when(distance(i) % 2 == 1)
        def _():
            kv_own(i).start()

    for u in range(UNITS):
        acc[u] = jnp.zeros_like(acc[u])
        peak[u] = jnp.full_like(peak[u], -1e30)
    for k in range(4):
        pltpu.make_async_copy(qown.at[0, 0], qb.at[k], qrecv.at[k]).wait()
    for i in range(2):

        @pl.when(distance(i) == 2)
        def _():
            kv_own(i).start()

    for chunk in range(12):
        tile, columns = chunk // 2, slice(128 * (chunk % 2), 128 * (chunk % 2) + 128)
        block = qb[chunk // 3, chunk % 3]
        zero = jnp.zeros((64, 128), BF)
        qm[0, tile, 0:64, columns] = block[0:64]
        qm[0, tile, 64:128, columns] = zero
        qm[1, tile, 0:64, columns] = zero
        qm[1, tile, 64:128, columns] = block[64:128]

    def score(u, keys, size):
        raw = jnp.dot(keys, qm[u % 2, u // 2], preferred_element_type=F32)
        sscr[u % (AHEAD + 1), 0:size, :] = raw
        tops[u % (AHEAD + 1)] = jnp.max(raw, axis=0, keepdims=True) * SCALE

    def weigh(u, lhs, size, bias):
        slot = u % (AHEAD + 1)
        top = tops[slot] if bias is None else tops[slot] + bias
        old = peak[u]
        new = jnp.maximum(old, top)
        peak[u] = new
        faded = jnp.exp2(old - new)
        shift = new if bias is None else new - bias
        probs = jnp.exp2(sscr[slot, 0:size, :] * SCALE - shift).astype(BF)
        acc[u] = acc[u] * faded + jnp.dot(lhs, probs, preferred_element_type=F32)

    def latent_keys(b):
        return kv[b, 0:OWN, :]

    def latent_lhs(b):
        lhs = jnp.concatenate([kv[b, OWN + 128 * a : OWN + 128 * a + 128, :] for a in range(6)], axis=1)
        return jnp.concatenate([lhs, jnp.ones((16, OWN), BF)], axis=0)

    def block_at(n):
        return sum((n == k).astype(jnp.int32) * source(*place) for k, place in enumerate(ORDER))

    arrive(s)
    keys, lhs = latent_keys(s), latent_lhs(s)
    for u in range(AHEAD):
        score(u, keys, OWN)
    for u in range(UNITS):
        if u + AHEAD < UNITS:
            score(u + AHEAD, keys, OWN)
        weigh(u, lhs, OWN, None)


    @pl.when(primary)
    def _():
        pass_on(*ORDER[1])

    @pl.when(jnp.logical_not(primary))
    def _():
        arrive(source(*ORDER[1]))

    keys = latent_keys(source(*ORDER[1]))
    for u in range(AHEAD):
        score(u, keys, OWN)

    def step(n, carry):
        for k, blocks in PASS.items():

            @pl.when(primary & (n == k))
            def _():
                for place in blocks:
                    pass_on(*place)

        following = block_at(jnp.minimum(n + 1, 15))

        @pl.when(jnp.logical_not(primary) & (n < 15))
        def _():
            arrive(following)

        @pl.when(n == 5)
        def _():
            for k in (1, 2):
                wcp[k].wait_recv()
                wcp[k + 4].start()
            for k in (3, 4):
                wcp[k].wait_recv()
                wcp[k + 4].start()

        @pl.when(n == 12)
        def _():
            wcp[5].wait_recv()
            wcp[6].wait_recv()
            wcp[9].start()

        b = block_at(n)
        keys, later, lhs = latent_keys(b), latent_keys(following), latent_lhs(b)
        for u in range(UNITS):
            if u + AHEAD < UNITS:
                score(u + AHEAD, keys, OWN)
            else:
                score(u + AHEAD - UNITS, later, OWN)
            weigh(u, lhs, OWN, None)
        return carry

    lax.fori_loop(1, 16, step, 0)

    lane = lax.broadcasted_iota(jnp.int32, (1, 128), 1)
    owner = y * 2 + z // 2

    def pick(row):
        return jnp.sum(jnp.where(lane == z % 2, mods[owner, row : row + 1, :], 0.0), axis=1, keepdims=True)

    bias, lam = pick(13) * LOG2E, pick(12)
    head = y * 4 + z
    half = 1 - primary.astype(jnp.int32)
    ocp = []
    for k in range(4):
        for e in range(4):
            offset = half if e // 2 == 0 else 3 * half + 3
            target = ((y + offset) % 4) * 2 + e % 2
            src = nsend.at[pl.ds(pl.multiple_of(384 * k + ROWS * e, 16), ROWS)]
            here = (k == z) & (target == t)
            ocp.append((src, k * 4 + x, target, here, 4 * k + e))

    for k in range(8):
        pair = jnp.concatenate([kv[2 * k, 2 * OWN + CTXR : BLOCK, :], kv[2 * k + 1, 2 * OWN + CTXR : BLOCK, :]], axis=0)
        vctx[:, 128 * k : 128 * k + 128] = pair.astype(F32).T.astype(BF)
    keys = jnp.concatenate([kv[k, 2 * OWN : 2 * OWN + CTXR, :] for k in range(16)], axis=0)
    lhs = jnp.concatenate([vctx[...], jnp.ones((16, 16 * CTXR), BF)], axis=0)
    size = 16 * CTXR
    for u in range(AHEAD):
        score(u, keys, size)
    pieces = 0
    for tile in range(NQ):
        for u in (2 * tile, 2 * tile + 1):
            if u + AHEAD < UNITS:
                score(u + AHEAD, keys, size)
            weigh(u, lhs, size, bias)
        one, two = acc[2 * tile], acc[2 * tile + 1]
        mixed = one[0:128] / one[128:129] - lam * (two[0:128] / two[128:129])
        normed = mixed * lax.rsqrt(jnp.mean(mixed * mixed, axis=0, keepdims=True) + EPS)
        for r in range(QT // 128):
            block = normed[:, 128 * r : 128 * r + 128].T * head_gain[...]
            row = QT * tile + 128 * r
            nsend[row : row + 128, :] = block.astype(BF)
        ready = QT * (tile + 1) // ROWS
        for src, sp, tp, here, index in ocp[pieces:ready]:

            @pl.when(here)
            def _():
                pltpu.make_async_copy(src, nrm.at[head], orecv.at[head]).start()

            @pl.when(jnp.logical_not(here))
            def _():
                remote(src, nrm.at[head], osend.at[index], orecv.at[head], sp, tp).start()

        pieces = ready

    attended = jnp.zeros((ROWS, 2048), F32)
    for p in range(4):
        group = ((y + (0, 3, 1, 2)[p]) % 4) * 2
        for k in {0: (0,), 1: (7,), 2: (8,), 3: (9,)}[p]:
            wcp[k].wait_recv()
        for k in range(4):
            pltpu.make_async_copy(nsend.at[0:ROWS], nrm.at[2 * group + k], orecv.at[2 * group + k]).wait()
        for k in range(2):
            rows = jnp.concatenate([nrm[2 * (group + k)], nrm[2 * (group + k) + 1]], axis=1)
            product = jnp.dot(rows, wall[p, 256 * k : 256 * k + 256, :], preferred_element_type=F32)
            attended = attended + product.astype(BF).astype(F32)
    rows = lat[0, pl.ds(pl.multiple_of(c * ROWS, 16), ROWS), :].astype(F32)
    out[...] = (rows + vector(2, 0) * attended.astype(BF).astype(F32)).astype(BF)

    for copy in lcp + wcp + mcp + ncp:
        copy.wait_send()
    for i in range(2):
        q_sib(i).wait_send()

        @pl.when(distance(i) != 0)
        def _():
            q_own(i).wait_send()
            kv_own(i).wait_send()

    @pl.when(primary)
    def _():
        for place in ORDER:
            for copy in onward(*place):
                copy.wait_send()

    for src, sp, tp, here, index in ocp:

        @pl.when(jnp.logical_not(here))
        def _():
            remote(src, nrm.at[head], osend.at[index], orecv.at[head], sp, tp).wait_send()


def per_device(
    latent, context, conditioning, norm_gain, mod_shift, mod_scale, mod_gate, w_query, w_key, w_value, w_out,
    lambdas, context_bias, head_gain,
):
    dma = pltpu.SemaphoreType.DMA
    vmem = pl.BlockSpec(memory_space=pltpu.VMEM)
    hbm = pl.BlockSpec(memory_space=pl.ANY)
    return pl.pallas_call(
        kernel,
        name="block",
        out_shape=jax.ShapeDtypeStruct(latent.shape, BF),
        in_specs=[hbm, hbm, vmem, vmem] + [hbm] * 7 + [vmem] * 3,
        out_specs=vmem,
        scratch_shapes=[
            pltpu.VMEM((4, PAIR, 2048), BF),
            pltpu.VMEM((CTXR, 2048), BF),
            pltpu.VMEM((3, 128, 256), BF),
            pltpu.VMEM((3, 2048, 256), BF),
            pltpu.VMEM((16, 16, 128), F32),
            pltpu.VMEM((16, 128), F32),
            pltpu.VMEM((16, 128), F32),
            pltpu.VMEM((8, 16, 128), F32),
            pltpu.VMEM((2, OWN, 256), F32),
            pltpu.VMEM((2, BLOCK, 128), BF),
            pltpu.VMEM((2, 2, 3, 128, 128), BF),
            pltpu.VMEM((16, BLOCK, 128), BF),
            pltpu.VMEM((4, 3, 128, 128), BF),
            pltpu.VMEM((2, NQ, 128, QT), BF),
            pltpu.VMEM((128, 16 * CTXR), BF),
            pltpu.VMEM((AHEAD + 1, 16 * CTXR, QT), F32),
            pltpu.VMEM((AHEAD + 1, 1, QT), F32),
            pltpu.VMEM((UNITS, 144, QT), F32),
            pltpu.VMEM((UNITS, 1, QT), F32),
            pltpu.VMEM((1536, 128), BF),
            pltpu.VMEM((16, ROWS, 128), BF),
            pltpu.VMEM((4, 512, 2048), BF),
            dma((10,)), dma((10,)), dma((10,)), dma((10,)),
            dma((16,)), dma((16,)), dma((8,)), dma((8,)),
            dma((2,)), dma((2, 2)), dma((16,)), dma((4,)),
            dma((16,)), dma((16,)), dma((16,)),
            dma((16,)), dma((16,)), dma((9,)),
        ],
        compiler_params=pltpu.CompilerParams(
            collective_id=0, has_side_effects=True, vmem_limit_bytes=60 * 2**20
        ),
    )(
        latent, context, conditioning, norm_gain.reshape(1, -1), mod_shift, mod_scale, mod_gate, w_query, w_key,
        w_value, w_out, lambdas.reshape(1, -1), context_bias.reshape(1, -1), head_gain.reshape(1, -1),
    )


def solution(mesh):
    return jax.shard_map(
        per_device,
        mesh=mesh,
        in_specs=(
            P(("sp", "tp"), None),
            P("sp", None),
            P(),
            P(),
            P("sp", "tp"),
            P("sp", "tp"),
            P("sp", "tp"),
            P(None, "tp"),
            P(None, "tp"),
            P(None, "tp"),
            P("tp", None),
            P("tp"),
            P("tp"),
            P(),
        ),
        out_specs=P(("sp", "tp"), None),
        check_vma=False,
    )
```

time: 110 us -> 95.8 us (0.87)
  Pallas kernels: 108 us -> 93.8 us
    pallas_call x1, Pallas kernels: 108 us -> 93.8 us  [per_device(): pl.pallas_call(kernel, name='block', out_shape=jax.ShapeDtypeStruct(laten...]
where the time goes in v2:
time: 95.8 us; the launch traced here: 95.6 us
  Pallas kernels  93.8 us (98%)
  local copies, waits for them, and re-layouts  1.77 us (2%)
    pallas_call x1, Pallas kernels, per_device(): pl.pallas_call(kernel, name='block', out_shape=jax.ShapeDtypeStruct(laten...  93.8 us

profile of v2, /device:TPU:1, one launch (start us, length us, event | category | flops | bytes accessed | tf_op | source)
XLA Modules:
  0.0 95.6 jit_solution(14377390329508720556)
XLA Ops:
  0.0 93.8 %block.1 = bf16[96,2048]{1,0:T(8,128)(2,1)} custom-call(bf16[96,2048]{1,0:T(8,128)(2,1)} %latent.1, bf16[64,2048]{1,0:T(8,128)(2,1)} %context.1, f32[2,2048]{1,0:T(2,128)} %cond.1, f32[1,2048]{1,0:T(1,128)} %bitcast.4, bf16[128,256]{1,0:T(8,128)(2,1)} %mod_shift.1, bf16[128,256]{1,0:T(8,128)(2,1)} %mod_scale.1, bf16[128,256]{1,0:T(8,128)(2,1)} %mod_gate.1, ...), custom_call_target="tpu_custom_call" | custom-call | tf_op jit(solution)/shard_map/block/pallas_call | solution.py:462
  93.8 1.8 %copy.16 = bf16[96,2048]{1,0:T(8,128)(2,1)} copy(bf16[96,2048]{1,0:T(8,128)(2,1)} %block.1) | data formatting | bytes 786432

commit v3 on v2

v3 whole, which is shorter than its diff:
```python
import functools
import math

import jax
import jax.numpy as jnp
from jax import lax
from jax.experimental import pallas as pl
from jax.experimental.pallas import tpu as pltpu
from jax.sharding import PartitionSpec as P

EPS = 1e-06
MESH = pl.DeviceIdType.MESH
BF = jnp.bfloat16
F32 = jnp.float32
LOG2E = math.log2(math.e)
SCALE = LOG2E / 8.0
ROWS = 96
PAIR = 192
OWN = 768
CTXR = 64
BLOCK = 2 * OWN + 2 * CTXR
QT = 256
NQ = 6
UNITS = 12
AHEAD = 3
ORDER = (
    (0, 0), (0, 1), (0, 3), (1, 0), (3, 0), (1, 1), (1, 3), (3, 1), (3, 3), (2, 0), (0, 2), (1, 2), (3, 2), (2, 1),
    (2, 3), (2, 2),
)
PACKED = tuple(sum(place[k] << 2 * (n % 8) for n, place in enumerate(ORDER[8 * h : 8 * h + 8])) for k in range(2) for h in range(2))
PASS = {
    0: ((0, 1, 0), (0, 1, 1), (0, 3, 0), (1, 0, 0), (3, 0, 0)), 1: ((0, 3, 1),), 2: ((1, 0, 1), (3, 0, 1)),
    4: ((1, 1, 0), (1, 1, 1), (1, 3, 0), (1, 3, 1)), 6: ((3, 1, 0), (3, 1, 1), (3, 3, 0), (3, 3, 1)),
    7: ((2, 0, 0), (2, 0, 1)), 8: ((0, 2, 0), (0, 2, 1)),
    10: ((1, 2, 0), (1, 2, 1), (3, 2, 0), (3, 2, 1), (2, 1, 0), (2, 1, 1)), 11: ((2, 3, 0), (2, 3, 1)),
    13: ((2, 2, 0), (2, 2, 1)),
}
HALF = OWN // 2
PARTS = ((0, OWN), (OWN, BLOCK - OWN))


def remote(src, dst, send, recv, sp, tp):
    return pltpu.make_async_remote_copy(
        src_ref=src, dst_ref=dst, send_sem=send, recv_sem=recv, device_id=(sp, tp), device_id_type=MESH
    )


def round_y(buf, rows, send, recv, s, y, c):
    up, down = ((y + 1) % 4) * 2 + c, ((y + 3) % 4) * 2 + c
    sib = y * 2 + 1 - c
    half = rows // 2

    def at(slot, offset, size):
        return buf.at[slot, pl.ds(pl.multiple_of(c * rows + offset, 16), size)]

    def one(k, source, slot, offset, size, to):
        return remote(at(source, offset, size), at(slot, offset, size), send.at[k], recv.at[k], s, to)

    return [
        one(0, 0, 0, 0, rows, sib),
        one(1, 0, 1, 0, half, up),
        one(2, 0, 2, half, half, down),
        one(3, 0, 1, half, half, up),
        one(4, 0, 2, 0, half, down),
        one(5, 1, 3, 0, half, up),
        one(6, 2, 3, half, half, down),
        one(7, 1, 1, 0, rows, sib),
        one(8, 2, 2, 0, rows, sib),
        one(9, 3, 3, 0, rows, sib),
    ]


def kernel(
    latent, context, cond, gain, mod_shift, mod_scale, mod_gate, w_query, w_key, w_value, w_out, lambdas,
    context_bias, head_gain, out,
    lat, ctx, mod, wqkv, part, msg, row, msg2, mods, qv, kvown, qown, kv, qb, qm, vctx, sscr, tops, acc, peak, nsend, nrm,
    wall, lsend, lrecv, wsend, wrecv, msend, mrecv, nsd, nrc, zsend, zqsend, kvrecv, qrecv, fsib, fplus, fminus,
    osend, orecv, local,
):
    s, t = lax.axis_index("sp"), lax.axis_index("tp")
    z, x, y, c = s // 4, s % 4, t // 2, t % 2
    sib = y * 2 + 1 - c

    barrier = pltpu.get_barrier_semaphore()
    for d in range(1, 8):
        pl.semaphore_signal(barrier, inc=1, device_id=(s, (t + d) % 8), device_id_type=MESH)
    for d in range(1, 4):
        pl.semaphore_signal(barrier, inc=1, device_id=(z * 4 + (x + d) % 4, t), device_id_type=MESH)
        pl.semaphore_signal(barrier, inc=1, device_id=((z + d) % 4 * 4 + x, t), device_id_type=MESH)
    loads = [
        pltpu.make_async_copy(src, dst, local.at[k])
        for k, (src, dst) in enumerate(
            (
                (mod_shift, mod.at[0]),
                (mod_scale, mod.at[1]),
                (mod_gate, mod.at[2]),
                (latent, lat.at[0, pl.ds(pl.multiple_of(c * ROWS, 16), ROWS)]),
                (context, ctx),
                (w_query, wqkv.at[0]),
                (w_key, wqkv.at[1]),
                (w_value, wqkv.at[2]),
                (w_out, wall.at[0, pl.ds(pl.multiple_of(c * 256, 256), 256)]),
            )
        )
    ]
    for copy in loads:
        copy.start()

    cols = cond[:, pl.ds(pl.multiple_of(s * 128, 128), 128)]
    activated = (cols / (1.0 + jnp.exp(-cols))).astype(BF)
    activated = jnp.concatenate([activated.astype(F32), jnp.zeros((6, 128), F32)], axis=0).astype(BF)
    msg[12:16, :] = jnp.zeros((4, 128), F32)
    for index in range(3):
        loads[index].wait()
        product = jnp.dot(activated, mod[index], preferred_element_type=F32)
        for r in range(2):
            for half in range(2):
                line = index * 4 + r * 2 + half
                msg[line : line + 1, :] = product[r : r + 1, half * 128 : half * 128 + 128]
    loads[3].wait()
    pl.semaphore_wait(barrier, 13)

    mcp = [
        remote(msg, part.at[0, x], msend.at[0, d], mrecv.at[0, d], z * 4 + (x + d) % 4, t) for d in range(1, 4)
    ]
    for copy in mcp:
        copy.start()
    lcp = round_y(lat, ROWS, lsend, lrecv, s, y, c)
    for k in (1, 2, 3, 4, 0):
        lcp[k].start()
    part[0, x] = msg[...]
    for copy in mcp:
        copy.wait_recv()
    row[...] = part[0, 0] + part[0, 1] + part[0, 2] + part[0, 3]
    zcp = [
        remote(row, part.at[1, z], msend.at[1, d], mrecv.at[1, d], (z + d) % 4 * 4 + x, t) for d in range(1, 4)
    ]
    for copy in zcp:
        copy.start()
    part[1, z] = row[...]
    for copy in zcp:
        copy.wait_recv()
    msg2[...] = part[1, 0] + part[1, 1] + part[1, 2] + part[1, 3]
    msg2[12:13, 0:2] = lambdas[...]
    msg2[13:14, 0:2] = context_bias[...]
    ncp = [remote(msg2, mods.at[t], nsd.at[d], nrc.at[d], s, (t + d) % 8) for d in range(1, 8)]
    for copy in ncp:
        copy.start()
    mods[t] = msg2[...]
    lcp[1].wait_recv()
    lcp[5].start()
    lcp[2].wait_recv()
    lcp[6].start()
    lcp[3].wait_recv()
    lcp[7].start()
    lcp[4].wait_recv()
    lcp[8].start()
    for copy in ncp:
        copy.wait_recv()

    def vector(index, r):
        row = index * 4 + r * 2
        return jnp.concatenate([mods[k, row + h : row + h + 1, :] for k in range(8) for h in range(2)], axis=1)

    def modulate(rows, r):
        rows = rows.astype(F32)
        normal = rows * lax.rsqrt(jnp.mean(rows * rows, axis=1, keepdims=True) + EPS)
        return (normal * (gain[...] * (1.0 + vector(1, r))) + vector(0, r)).astype(BF)

    def project(p):
        hidden = modulate(lat[p], 0)
        rows = slice(PAIR * p, PAIR * p + PAIR)
        first = PAIR * p + HALF * (p // 2)
        qv[0, rows, :] = jnp.dot(hidden, wqkv[0], preferred_element_type=F32)
        keys = jnp.dot(hidden, wqkv[1], preferred_element_type=F32).astype(BF)
        for i in range(2):
            kvown[i, first : first + PAIR, :] = keys[:, 128 * i : 128 * i + 128]
        qv[1, rows, :] = jnp.dot(hidden, wqkv[2], preferred_element_type=F32)

    for copy in loads[4:]:
        copy.wait()
    hidden = modulate(ctx[...], 1)
    keys = jnp.dot(hidden, wqkv[1], preferred_element_type=F32).astype(BF)
    values = jnp.dot(hidden, wqkv[2], preferred_element_type=F32).astype(BF)
    for i in range(2):
        kvown[i, 2 * OWN : 2 * OWN + CTXR, :] = keys[:, 128 * i : 128 * i + 128]
        kvown[i, 2 * OWN + CTXR : BLOCK, :] = values[:, 128 * i : 128 * i + 128]
    lcp[0].wait_recv()
    project(0)
    lcp[7].wait_recv()
    project(1)

    primary = c == z // 2
    plus, minus = z * 4 + (x + 1) % 4, z * 4 + (x + 3) % 4

    def turn(part):
        for a in range(3 * part, 3 * part + 3):
            for i in range(2):
                rows, columns = slice(128 * a, 128 * a + 128), slice(128 * i, 128 * i + 128)
                qown[part, i, a % 3] = qv[0, rows, columns].T.astype(BF)
                first = OWN * part + HALF + 128 * (a % 3)
                kvown[i, first : first + 128, :] = qv[1, rows, columns].T.astype(BF)

    def distance(i):
        return (2 * c + i - z + 4) % 4

    def slot_of(dz):
        return 3 * (dz == 0).astype(jnp.int32) + (dz == 1).astype(jnp.int32) + 2 * (dz == 3).astype(jnp.int32)

    def q_to(i, part):
        slot = slot_of((z - 2 * c - i + 4) % 4)
        return remote(
            qown.at[part, i], qb.at[slot], zqsend.at[i, part], qrecv.at[slot], (2 * c + i) * 4 + x, sib if part else t
        )

    def part_of(ref, b, part):
        return ref.at[b, pl.ds(*PARTS[part])]

    def kv_to(i, part):
        return remote(
            part_of(kvown, i, part), part_of(kv, s, part), zsend.at[i, part], kvrecv.at[part, s],
            (2 * c + i) * 4 + x, t,
        )

    def source(dz, dx):
        return ((z + dz) % 4) * 4 + (x + dx) % 4

    def onward(dz, dx, part):
        b = source(dz, dx)
        src = part_of(kvown, z % 2, part) if (dz, dx) == (0, 0) else part_of(kv, b, part)
        dst = part_of(kv, b, part)
        copies = []
        if dx == 0 or (dx == 3 and dz < 2):
            copies.append(remote(src, dst, fplus.at[part, b], kvrecv.at[part, b], plus, t))
        if dx == 0 or (dx == 1 and dz >= 2):
            copies.append(remote(src, dst, fminus.at[part, b], kvrecv.at[part, b], minus, t))
        copies.append(remote(src, dst, fsib.at[part, b], kvrecv.at[part, b], s, sib))
        return copies

    def arrive(b, part):
        pltpu.make_async_copy(part_of(kvown, 0, part), part_of(kv, b, part), kvrecv.at[part, b]).wait()

    def pass_on(dz, dx, part):
        arrive(source(dz, dx), part)
        for copy in onward(dz, dx, part):
            copy.start()

    def send_part(part):
        for i in range(2):
            if part:
                q_to(i, 1).start()

            @pl.when(distance(i) != 0)
            def _():
                if not part:
                    q_to(i, 0).start()

            @pl.when(distance(i) == 0)
            def _():
                if not part:
                    pltpu.make_async_copy(qown.at[0, i], qb.at[3], qrecv.at[3]).start()
                pltpu.make_async_copy(part_of(kvown, i, part), part_of(kv, s, part), kvrecv.at[part, s]).start()

        @pl.when(primary)
        def _():
            for copy in onward(0, 0, part):
                copy.start()

        for i in range(2):

            @pl.when(distance(i) % 2 == 1)
            def _():
                kv_to(i, part).start()

    def send_far(part):
        for i in range(2):

            @pl.when(distance(i) == 2)
            def _():
                kv_to(i, part).start()

    turn(0)
    send_part(0)
    lcp[5].wait_recv()
    lcp[6].wait_recv()
    lcp[9].start()
    lcp[8].wait_recv()
    project(2)
    lcp[9].wait_recv()
    project(3)
    turn(1)
    send_part(1)
    wcp = round_y(wall, 256, wsend, wrecv, s, y, c)
    for k in (1, 2, 3, 4, 0):
        wcp[k].start()

    for u in range(UNITS):
        acc[u] = jnp.zeros_like(acc[u])
        peak[u] = jnp.full_like(peak[u], -1e30)
    for k in range(4):
        pltpu.make_async_copy(qown.at[0, 0], qb.at[k], qrecv.at[k]).wait()

    for chunk in range(12):
        tile, columns = chunk // 2, slice(128 * (chunk % 2), 128 * (chunk % 2) + 128)
        block = qb[chunk // 3, chunk % 3]
        zero = jnp.zeros((64, 128), BF)
        qm[0, tile, 0:64, columns] = block[0:64]
        qm[0, tile, 64:128, columns] = zero
        qm[1, tile, 0:64, columns] = zero
        qm[1, tile, 64:128, columns] = block[64:128]

    def score(u, at, keys, size):
        raw = jnp.dot(keys, qm[u % 2, u // 2], preferred_element_type=F32)
        sscr[at % (AHEAD + 1), 0:size, :] = raw
        tops[at % (AHEAD + 1)] = jnp.max(raw, axis=0, keepdims=True) * SCALE

    def weigh(u, at, lhs, size, bias):
        slot = at % (AHEAD + 1)
        top = tops[slot] if bias is None else tops[slot] + bias
        old = peak[u]
        new = jnp.maximum(old, top)
        peak[u] = new
        faded = jnp.exp2(old - new)
        shift = new if bias is None else new - bias
        probs = jnp.exp2(sscr[slot, 0:size, :] * SCALE - shift).astype(BF)
        acc[u] = acc[u] * faded + jnp.dot(lhs, probs, preferred_element_type=F32)

    def latent_keys(b):
        return jnp.concatenate([kv[b, 0:HALF, :], kv[b, OWN : OWN + HALF, :]], axis=0)

    def latent_lhs(b):
        lhs = jnp.concatenate([kv[b, k : k + 128, :] for a in (HALF, OWN + HALF) for k in range(a, a + HALF, 128)], axis=1)
        return jnp.concatenate([lhs, jnp.ones((16, OWN), BF)], axis=0)

    def block_at(n):
        late = (n >= 8).astype(jnp.int32)
        by = 2 * (n - 8 * late)
        dz = ((PACKED[0] * (1 - late) + PACKED[1] * late) >> by) % 4
        dx = ((PACKED[2] * (1 - late) + PACKED[3] * late) >> by) % 4
        return source(dz, dx)

    arrive(s, 0)
    arrive(s, 1)
    keys, lhs = latent_keys(s), latent_lhs(s)
    for u in range(AHEAD):
        score(u, u, keys, OWN)
    for u in range(UNITS):
        if u + AHEAD < UNITS:
            score(u + AHEAD, u + AHEAD, keys, OWN)
        weigh(u, u, lhs, OWN, None)


    @pl.when(primary)
    def _():
        for place in PASS[0]:
            pass_on(*place)

    @pl.when(jnp.logical_not(primary))
    def _():
        arrive(source(0, 1), 0)
        arrive(source(0, 1), 1)

    keys = latent_keys(source(0, 1))
    for u in range(AHEAD):
        score(u, u, keys, OWN)

    def step(n, b):
        following = block_at(n + 1)

        @pl.when(primary)
        def _():
            for steps in ((1, 2, 4), (6, 7, 8), (10, 11, 13)):

                @pl.when((n >= steps[0]) & (n <= steps[-1]))
                def _():
                    for k in steps:

                        @pl.when(n == k)
                        def _():
                            for place in PASS[k]:
                                pass_on(*place)

        @pl.when(jnp.logical_not(primary))
        def _():
            arrive(following, 0)
            arrive(following, 1)

        @pl.when(n == 2)
        def _():
            send_far(0)
            send_far(1)

        @pl.when(n == 7)
        def _():
            for k in (1, 2):
                wcp[k].wait_recv()
                wcp[k + 4].start()
            for k in (3, 4):
                wcp[k].wait_recv()
                wcp[k + 4].start()

        @pl.when(n == 13)
        def _():
            wcp[5].wait_recv()
            wcp[6].wait_recv()
            wcp[9].start()

        keys, later, lhs = latent_keys(b), latent_keys(following), latent_lhs(b)
        for u in range(UNITS):
            if u + AHEAD < UNITS:
                score(u + AHEAD, u + AHEAD, keys, OWN)
            else:
                score(u + AHEAD - UNITS, u + AHEAD, later, OWN)
            weigh(u, u, lhs, OWN, None)
        return following

    last = lax.fori_loop(1, 15, step, source(0, 1))

    lane = lax.broadcasted_iota(jnp.int32, (1, 128), 1)
    owner = y * 2 + z // 2

    def pick(row):
        return jnp.sum(jnp.where(lane == z % 2, mods[owner, row : row + 1, :], 0.0), axis=1, keepdims=True)

    bias, lam = pick(13) * LOG2E, pick(12)
    head = y * 4 + z
    half = 1 - primary.astype(jnp.int32)

    def piece(k):
        offset = half if k % 4 // 2 == 0 else 3 * half + 3
        target = ((y + offset) % 4) * 2 + k % 2
        src = nsend.at[ROWS * k : ROWS * k + ROWS]
        return remote(src, nrm.at[head], osend.at[k], orecv.at[head], ((z + (2, 1, 3, 0)[k // 4]) % 4) * 4 + x, target)

    for k in range(8):
        pair = jnp.concatenate([kv[2 * k, 2 * OWN + CTXR : BLOCK, :], kv[2 * k + 1, 2 * OWN + CTXR : BLOCK, :]], axis=0)
        vctx[:, 128 * k : 128 * k + 128] = pair.astype(F32).T.astype(BF)
    size = 16 * CTXR
    keys = (latent_keys(last), jnp.concatenate([kv[k, 2 * OWN : 2 * OWN + CTXR, :] for k in range(16)], axis=0))
    lhs = (latent_lhs(last), jnp.concatenate([vctx[...], jnp.ones((16, size), BF)], axis=0))
    sizes, biases = (OWN, size), (None, bias)
    turns = [(0, u) for u in range(4)]
    for u in range(0, UNITS, 2):
        turns += [(1, u), (1, u + 1)]
        turns += [(0, u + 4), (0, u + 5)] if u + 5 < UNITS else []
    pieces = 0
    for k, (which, u) in enumerate(turns):
        if k + AHEAD < len(turns):
            other, v = turns[k + AHEAD]
            score(v, k + AHEAD, keys[other], sizes[other])
        weigh(u, k, lhs[which], sizes[which], biases[which])
        if which == 0 or u % 2 == 0:
            continue
        tile = u // 2
        one, two = acc[2 * tile], acc[2 * tile + 1]
        mixed = one[0:128] / one[128:129] - lam * (two[0:128] / two[128:129])
        normed = mixed * lax.rsqrt(jnp.mean(mixed * mixed, axis=0, keepdims=True) + EPS)
        for r in range(QT // 128):
            block = normed[:, 128 * r : 128 * r + 128].T * head_gain[...]
            row = QT * tile + 128 * r
            nsend[row : row + 128, :] = block.astype(BF)
        if tile % 2 == 0:
            continue
        ready = QT * (tile + 1) // ROWS
        for e in range(pieces, ready):
            if e not in (12, 13):
                piece(e).start()
                continue
            mine = primary & (c == e - 12)

            @pl.when(mine)
            def _():
                src = nsend.at[ROWS * e : ROWS * e + ROWS]
                pltpu.make_async_copy(src, nrm.at[head], orecv.at[head]).start()

            @pl.when(jnp.logical_not(mine))
            def _():
                piece(e).start()

        pieces = ready

    for k in (0, 7, 8, 9):
        wcp[k].wait_recv()
    attended = jnp.zeros((ROWS, 2048), F32)
    for k in (1 - z // 2, z // 2):
        for p in range(4):
            first = 4 * ((y + (0, 3, 1, 2)[p]) % 4) + 2 * k
            for h in (first, first + 1):
                pltpu.make_async_copy(nsend.at[0:ROWS], nrm.at[h], orecv.at[h]).wait()
            rows = jnp.concatenate([nrm[first], nrm[first + 1]], axis=1)
            part_of_w = wall[p, pl.ds(pl.multiple_of(256 * k, 256), 256), :]
            product = jnp.dot(rows, part_of_w, preferred_element_type=F32)
            attended = attended + product.astype(BF).astype(F32)
    rows = lat[0, pl.ds(pl.multiple_of(c * ROWS, 16), ROWS), :].astype(F32)
    out[...] = (rows + vector(2, 0) * attended.astype(BF).astype(F32)).astype(BF)

    for copy in lcp + wcp + mcp + zcp + ncp:
        copy.wait_send()
    for i in range(2):
        q_to(i, 1).wait_send()

        @pl.when(distance(i) != 0)
        def _():
            q_to(i, 0).wait_send()
            for part in range(2):
                kv_to(i, part).wait_send()

    @pl.when(primary)
    def _():
        for place in ORDER:
            for part in range(2):
                for copy in onward(*place, part):
                    copy.wait_send()

    for e in range(16):
        if e not in (12, 13):
            piece(e).wait_send()
            continue

        @pl.when(jnp.logical_not(primary & (c == e - 12)))
        def _():
            piece(e).wait_send()


def per_device(
    latent, context, conditioning, norm_gain, mod_shift, mod_scale, mod_gate, w_query, w_key, w_value, w_out,
    lambdas, context_bias, head_gain,
):
    dma = pltpu.SemaphoreType.DMA
    vmem = pl.BlockSpec(memory_space=pltpu.VMEM)
    hbm = pl.BlockSpec(memory_space=pl.ANY)
    return pl.pallas_call(
        kernel,
        name="block",
        out_shape=jax.ShapeDtypeStruct(latent.shape, BF),
        in_specs=[hbm, hbm, vmem, vmem] + [hbm] * 7 + [vmem] * 3,
        out_specs=vmem,
        scratch_shapes=[
            pltpu.VMEM((4, PAIR, 2048), BF),
            pltpu.VMEM((CTXR, 2048), BF),
            pltpu.VMEM((3, 128, 256), BF),
            pltpu.VMEM((3, 2048, 256), BF),
            pltpu.VMEM((2, 4, 16, 128), F32),
            pltpu.VMEM((16, 128), F32),
            pltpu.VMEM((16, 128), F32),
            pltpu.VMEM((16, 128), F32),
            pltpu.VMEM((8, 16, 128), F32),
            pltpu.VMEM((2, OWN, 256), F32),
            pltpu.VMEM((2, BLOCK, 128), BF),
            pltpu.VMEM((2, 2, 3, 128, 128), BF),
            pltpu.VMEM((16, BLOCK, 128), BF),
            pltpu.VMEM((4, 3, 128, 128), BF),
            pltpu.VMEM((2, NQ, 128, QT), BF),
            pltpu.VMEM((128, 16 * CTXR), BF),
            pltpu.VMEM((AHEAD + 1, 16 * CTXR, QT), F32),
            pltpu.VMEM((AHEAD + 1, 1, QT), F32),
            pltpu.VMEM((UNITS, 144, QT), F32),
            pltpu.VMEM((UNITS, 1, QT), F32),
            pltpu.VMEM((1536, 128), BF),
            pltpu.VMEM((16, ROWS, 128), BF),
            pltpu.VMEM((4, 512, 2048), BF),
            dma((10,)), dma((10,)), dma((10,)), dma((10,)),
            dma((2, 4)), dma((2, 4)), dma((8,)), dma((8,)),
            dma((2, 2)), dma((2, 2)), dma((2, 16)), dma((4,)),
            dma((2, 16)), dma((2, 16)), dma((2, 16)),
            dma((16,)), dma((16,)), dma((9,)),
        ],
        compiler_params=pltpu.CompilerParams(
            collective_id=0, has_side_effects=True, vmem_limit_bytes=60 * 2**20
        ),
    )(
        latent, context, conditioning, norm_gain.reshape(1, -1), mod_shift, mod_scale, mod_gate, w_query, w_key,
        w_value, w_out, lambdas.reshape(1, -1), context_bias.reshape(1, -1), head_gain.reshape(1, -1),
    )


def solution(mesh):
    return jax.shard_map(
        per_device,
        mesh=mesh,
        in_specs=(
            P(("sp", "tp"), None),
            P("sp", None),
            P(),
            P(),
            P("sp", "tp"),
            P("sp", "tp"),
            P("sp", "tp"),
            P(None, "tp"),
            P(None, "tp"),
            P(None, "tp"),
            P("tp", None),
            P("tp"),
            P("tp"),
            P(),
        ),
        out_specs=P(("sp", "tp"), None),
        check_vma=False,
    )
```

time: 95.8 us -> 89.4 us (0.933)
  Pallas kernels: 93.8 us -> 87.4 us
    pallas_call x1, Pallas kernels: 93.8 us -> 87.4 us  [per_device(): pl.pallas_call(kernel, name='block', out_shape=jax.ShapeDtypeStruct(laten...]
where the time goes in v3:
time: 89.4 us; the launch traced here: 89.2 us
  Pallas kernels  87.4 us (98%)
  local copies, waits for them, and re-layouts  1.77 us (2%)
    pallas_call x1, Pallas kernels, per_device(): pl.pallas_call(kernel, name='block', out_shape=jax.ShapeDtypeStruct(laten...  87.4 us

profile of v3, /device:TPU:1, one launch (start us, length us, event | category | flops | bytes accessed | tf_op | source)
XLA Modules:
  0.0 89.2 jit_solution(17697961892285491136)
XLA Ops:
  0.0 87.4 %block.1 = bf16[96,2048]{1,0:T(8,128)(2,1)} custom-call(bf16[96,2048]{1,0:T(8,128)(2,1)} %latent.1, bf16[64,2048]{1,0:T(8,128)(2,1)} %context.1, f32[2,2048]{1,0:T(2,128)} %cond.1, f32[1,2048]{1,0:T(1,128)} %bitcast.4, bf16[128,256]{1,0:T(8,128)(2,1)} %mod_shift.1, bf16[128,256]{1,0:T(8,128)(2,1)} %mod_scale.1, bf16[128,256]{1,0:T(8,128)(2,1)} %mod_gate.1, ...), custom_call_target="tpu_custom_call" | custom-call | tf_op jit(solution)/shard_map/block/pallas_call | solution.py:532
  87.4 1.8 %copy.16 = bf16[96,2048]{1,0:T(8,128)(2,1)} copy(bf16[96,2048]{1,0:T(8,128)(2,1)} %block.1) | data formatting | bytes 786432

commit v4 on v3

--- a/solution.py
+++ b/solution.py
@@ -24,16 +24,23 @@
 UNITS = 12
 AHEAD = 3
 ORDER = (
-    (0, 0), (0, 1), (0, 3), (1, 0), (3, 0), (1, 1), (1, 3), (3, 1), (3, 3), (2, 0), (0, 2), (1, 2), (3, 2), (2, 1),
+    (0, 0), (0, 1), (0, 3), (1, 0), (3, 0), (0, 2), (1, 1), (1, 3), (3, 1), (3, 3), (2, 0), (1, 2), (2, 1), (3, 2),
     (2, 3), (2, 2),
 )
 PACKED = tuple(sum(place[k] << 2 * (n % 8) for n, place in enumerate(ORDER[8 * h : 8 * h + 8])) for k in range(2) for h in range(2))
 PASS = {
-    0: ((0, 1, 0), (0, 1, 1), (0, 3, 0), (1, 0, 0), (3, 0, 0)), 1: ((0, 3, 1),), 2: ((1, 0, 1), (3, 0, 1)),
-    4: ((1, 1, 0), (1, 1, 1), (1, 3, 0), (1, 3, 1)), 6: ((3, 1, 0), (3, 1, 1), (3, 3, 0), (3, 3, 1)),
-    7: ((2, 0, 0), (2, 0, 1)), 8: ((0, 2, 0), (0, 2, 1)),
-    10: ((1, 2, 0), (1, 2, 1), (3, 2, 0), (3, 2, 1), (2, 1, 0), (2, 1, 1)), 11: ((2, 3, 0), (2, 3, 1)),
-    13: ((2, 2, 0), (2, 2, 1)),
+    0: ((0, 1, 0, 0), (0, 1, 1, 0), (0, 3, 0, 0)),
+    1: ((0, 3, 1, 0),),
+    2: ((1, 0, 0, 0), (1, 0, 1, 0), (3, 0, 0, 0), (3, 0, 1, 0)),
+    4: ((0, 2, 0, 0), (0, 2, 1, 0)),
+    5: ((1, 1, 0, 0), (1, 1, 1, 0)),
+    6: ((1, 3, 0, 0), (1, 3, 1, 0), (2, 0, 0, 0), (2, 0, 1, 0)),
+    7: ((3, 1, 0, 0), (3, 1, 1, 0)),
+    8: ((3, 3, 0, 0), (3, 3, 1, 0)),
+    10: ((1, 2, 0, 0), (1, 2, 1, 0), (2, 1, 0, 0), (2, 1, 1, 0)),
+    11: ((3, 2, 0, 0), (3, 2, 1, 0)),
+    12: ((2, 3, 0, 0), (2, 3, 1, 0)),
+    14: ((2, 2, 0, 0), (2, 2, 1, 0)),
 }
 HALF = OWN // 2
 PARTS = ((0, OWN), (OWN, BLOCK - OWN))
@@ -73,9 +80,9 @@
 def kernel(
     latent, context, cond, gain, mod_shift, mod_scale, mod_gate, w_query, w_key, w_value, w_out, lambdas,
     context_bias, head_gain, out,
-    lat, ctx, mod, wqkv, part, msg, row, msg2, mods, qv, kvown, qown, kv, qb, qm, vctx, sscr, tops, acc, peak, nsend, nrm,
+    lat, ctx, mod, wqkv, part, msg, msg2, mods, qv, kvown, qown, kv, qb, qm, vctx, sscr, tops, acc, peak, nsend, nrm,
     wall, lsend, lrecv, wsend, wrecv, msend, mrecv, nsd, nrc, zsend, zqsend, kvrecv, qrecv, fsib, fplus, fminus,
-    osend, orecv, local,
+    osend, orecv, local, ready,
 ):
     s, t = lax.axis_index("sp"), lax.axis_index("tp")
     z, x, y, c = s // 4, s % 4, t // 2, t % 2
@@ -120,27 +127,22 @@
     loads[3].wait()
     pl.semaphore_wait(barrier, 13)
 
-    mcp = [
-        remote(msg, part.at[0, x], msend.at[0, d], mrecv.at[0, d], z * 4 + (x + d) % 4, t) for d in range(1, 4)
-    ]
-    for copy in mcp:
-        copy.start()
     lcp = round_y(lat, ROWS, lsend, lrecv, s, y, c)
     for k in (1, 2, 3, 4, 0):
         lcp[k].start()
-    part[0, x] = msg[...]
+    for d in range(1, 4):
+        pl.semaphore_signal(ready, inc=1, device_id=((z + d) % 4 * 4 + x, t), device_id_type=MESH)
+    pl.semaphore_wait(ready, 3)
+    mcp = [remote(msg, part.at[s], msend.at[d], mrecv.at[d], (s + d) % 16, t) for d in range(1, 16)]
+    for copy in mcp:
+        copy.start()
+    part[s] = msg[...]
     for copy in mcp:
         copy.wait_recv()
-    row[...] = part[0, 0] + part[0, 1] + part[0, 2] + part[0, 3]
-    zcp = [
-        remote(row, part.at[1, z], msend.at[1, d], mrecv.at[1, d], (z + d) % 4 * 4 + x, t) for d in range(1, 4)
-    ]
-    for copy in zcp:
-        copy.start()
-    part[1, z] = row[...]
-    for copy in zcp:
-        copy.wait_recv()
-    msg2[...] = part[1, 0] + part[1, 1] + part[1, 2] + part[1, 3]
+    total = part[0]
+    for k in range(1, 16):
+        total = total + part[k]
+    msg2[...] = total
     msg2[12:13, 0:2] = lambdas[...]
     msg2[13:14, 0:2] = context_bias[...]
     ncp = [remote(msg2, mods.at[t], nsd.at[d], nrc.at[d], s, (t + d) % 8) for d in range(1, 8)]
@@ -240,10 +242,12 @@
     def arrive(b, part):
         pltpu.make_async_copy(part_of(kvown, 0, part), part_of(kv, b, part), kvrecv.at[part, b]).wait()
 
-    def pass_on(dz, dx, part):
-        arrive(source(dz, dx), part)
+    def pass_on(dz, dx, part, how):
+        if how < 2:
+            arrive(source(dz, dx), part)
         for copy in onward(dz, dx, part):
-            copy.start()
+            if how == 0 or (how == 1) == (copy.device_id[1] is sib):
+                copy.start()
 
     def send_part(part):
         for i in range(2):
@@ -266,11 +270,13 @@
             for copy in onward(0, 0, part):
                 copy.start()
 
-        for i in range(2):
-
-            @pl.when(distance(i) % 2 == 1)
-            def _():
-                kv_to(i, part).start()
+        if part:
+            for i in range(2):
+
+                @pl.when(distance(i) % 2 == 1)
+                def _():
+                    kv_to(i, 0).start()
+                    kv_to(i, 1).start()
 
     def send_far(part):
         for i in range(2):
@@ -369,7 +375,7 @@
 
         @pl.when(primary)
         def _():
-            for steps in ((1, 2, 4), (6, 7, 8), (10, 11, 13)):
+            for steps in ((1, 2, 4), (5, 6, 7), (8, 10, 11), (12, 14)):
 
                 @pl.when((n >= steps[0]) & (n <= steps[-1]))
                 def _():
@@ -385,7 +391,7 @@
             arrive(following, 0)
             arrive(following, 1)
 
-        @pl.when(n == 2)
+        @pl.when(n == 1)
         def _():
             send_far(0)
             send_far(1)
@@ -459,7 +465,7 @@
             block = normed[:, 128 * r : 128 * r + 128].T * head_gain[...]
             row = QT * tile + 128 * r
             nsend[row : row + 128, :] = block.astype(BF)
-        if tile % 2 == 0:
+        if tile in (0, 2):
             continue
         ready = QT * (tile + 1) // ROWS
         for e in range(pieces, ready):
@@ -483,10 +489,11 @@
         wcp[k].wait_recv()
     attended = jnp.zeros((ROWS, 2048), F32)
     for k in (1 - z // 2, z // 2):
-        for p in range(4):
-            first = 4 * ((y + (0, 3, 1, 2)[p]) % 4) + 2 * k
+        firsts = [4 * ((y + off) % 4) + 2 * k for off in (0, 3, 1, 2)]
+        for first in firsts:
             for h in (first, first + 1):
                 pltpu.make_async_copy(nsend.at[0:ROWS], nrm.at[h], orecv.at[h]).wait()
+        for p, first in enumerate(firsts):
             rows = jnp.concatenate([nrm[first], nrm[first + 1]], axis=1)
             part_of_w = wall[p, pl.ds(pl.multiple_of(256 * k, 256), 256), :]
             product = jnp.dot(rows, part_of_w, preferred_element_type=F32)
@@ -494,7 +501,7 @@
     rows = lat[0, pl.ds(pl.multiple_of(c * ROWS, 16), ROWS), :].astype(F32)
     out[...] = (rows + vector(2, 0) * attended.astype(BF).astype(F32)).astype(BF)
 
-    for copy in lcp + wcp + mcp + zcp + ncp:
+    for copy in lcp + wcp + mcp + ncp:
         copy.wait_send()
     for i in range(2):
         q_to(i, 1).wait_send()
@@ -540,8 +547,7 @@
             pltpu.VMEM((CTXR, 2048), BF),
             pltpu.VMEM((3, 128, 256), BF),
             pltpu.VMEM((3, 2048, 256), BF),
-            pltpu.VMEM((2, 4, 16, 128), F32),
-            pltpu.VMEM((16, 128), F32),
+            pltpu.VMEM((16, 16, 128), F32),
             pltpu.VMEM((16, 128), F32),
             pltpu.VMEM((16, 128), F32),
             pltpu.VMEM((8, 16, 128), F32),
@@ -560,10 +566,11 @@
             pltpu.VMEM((16, ROWS, 128), BF),
             pltpu.VMEM((4, 512, 2048), BF),
             dma((10,)), dma((10,)), dma((10,)), dma((10,)),
-            dma((2, 4)), dma((2, 4)), dma((8,)), dma((8,)),
+            dma((16,)), dma((16,)), dma((8,)), dma((8,)),
             dma((2, 2)), dma((2, 2)), dma((2, 16)), dma((4,)),
             dma((2, 16)), dma((2, 16)), dma((2, 16)),
             dma((16,)), dma((16,)), dma((9,)),
+            pltpu.SemaphoreType.REGULAR,
         ],
         compiler_params=pltpu.CompilerParams(
             collective_id=0, has_side_effects=True, vmem_limit_bytes=60 * 2**20

time: 89.4 us -> 87.4 us (0.978)
  Pallas kernels: 87.4 us -> 85.4 us
    pallas_call x1, Pallas kernels: 87.4 us -> 85.4 us  [per_device(): pl.pallas_call(kernel, name='block', out_shape=jax.ShapeDtypeStruct(laten...]
where the time goes in v4:
time: 87.4 us; the launch traced here: 87.2 us
  Pallas kernels  85.4 us (98%)
  local copies, waits for them, and re-layouts  1.77 us (2%)
    pallas_call x1, Pallas kernels, per_device(): pl.pallas_call(kernel, name='block', out_shape=jax.ShapeDtypeStruct(laten...  85.4 us
    unnamed x1, local copies, waits for them, and re-layouts  1.77 us

profile of v4, /device:TPU:1, one launch (start us, length us, event | category | flops | bytes accessed | tf_op | source)
XLA Modules:
  0.0 87.2 jit_solution(10647780788856337449)
XLA Ops:
  0.0 85.4 %block.1 = bf16[96,2048]{1,0:T(8,128)(2,1)} custom-call(bf16[96,2048]{1,0:T(8,128)(2,1)} %latent.1, bf16[64,2048]{1,0:T(8,128)(2,1)} %context.1, f32[2,2048]{1,0:T(2,128)} %cond.1, f32[1,2048]{1,0:T(1,128)} %bitcast.4, bf16[128,256]{1,0:T(8,128)(2,1)} %mod_shift.1, bf16[128,256]{1,0:T(8,128)(2,1)} %mod_scale.1, bf16[128,256]{1,0:T(8,128)(2,1)} %mod_gate.1, ...), custom_call_target="tpu_custom_call" | custom-call | tf_op jit(solution)/shard_map/block/pallas_call | solution.py:539
  85.4 1.8 %copy.16 = bf16[96,2048]{1,0:T(8,128)(2,1)} copy(bf16[96,2048]{1,0:T(8,128)(2,1)} %block.1) | data formatting | bytes 786432

commit v5 on v4

--- a/solution.py
+++ b/solution.py
@@ -23,24 +23,20 @@
 NQ = 6
 UNITS = 12
 AHEAD = 3
-ORDER = (
-    (0, 0), (0, 1), (0, 3), (1, 0), (3, 0), (0, 2), (1, 1), (1, 3), (3, 1), (3, 3), (2, 0), (1, 2), (2, 1), (3, 2),
-    (2, 3), (2, 2),
+FIRST = (
+    (0, 0), (0, 1), (1, 0), (0, 1), (1, 0), (0, 2), (1, 1), (1, 3), (3, 1), (3, 3), (2, 0), (1, 2), (2, 1), (2, 3),
+    (3, 2), (2, 2),
 )
-PACKED = tuple(sum(place[k] << 2 * (n % 8) for n, place in enumerate(ORDER[8 * h : 8 * h + 8])) for k in range(2) for h in range(2))
+SECOND = (FIRST[0], (0, 3), (3, 0), (0, 3), (3, 0)) + FIRST[5:]
+PACKED = tuple(
+    tuple(sum(place[k] << 2 * n for n, place in enumerate(order[8 * word : 8 * word + 8])) for word in range(2))
+    for order in (FIRST, SECOND)
+    for k in range(2)
+)
 PASS = {
-    0: ((0, 1, 0, 0), (0, 1, 1, 0), (0, 3, 0, 0)),
-    1: ((0, 3, 1, 0),),
-    2: ((1, 0, 0, 0), (1, 0, 1, 0), (3, 0, 0, 0), (3, 0, 1, 0)),
-    4: ((0, 2, 0, 0), (0, 2, 1, 0)),
-    5: ((1, 1, 0, 0), (1, 1, 1, 0)),
-    6: ((1, 3, 0, 0), (1, 3, 1, 0), (2, 0, 0, 0), (2, 0, 1, 0)),
-    7: ((3, 1, 0, 0), (3, 1, 1, 0)),
-    8: ((3, 3, 0, 0), (3, 3, 1, 0)),
-    10: ((1, 2, 0, 0), (1, 2, 1, 0), (2, 1, 0, 0), (2, 1, 1, 0)),
-    11: ((3, 2, 0, 0), (3, 2, 1, 0)),
-    12: ((2, 3, 0, 0), (2, 3, 1, 0)),
-    14: ((2, 2, 0, 0), (2, 2, 1, 0)),
+    3: ((1, 0, 1), (3, 0, 1)), 4: ((0, 2, 0), (0, 2, 1)), 5: ((1, 1, 0), (1, 1, 1)), 6: ((1, 3, 0), (1, 3, 1)),
+    7: ((2, 0, 0), (2, 0, 1), (3, 1, 0), (3, 1, 1)), 8: ((3, 3, 0), (3, 3, 1)), 10: ((1, 2, 0), (1, 2, 1)),
+    11: ((2, 1, 0), (2, 1, 1)), 12: ((2, 3, 0), (2, 3, 1)), 13: ((3, 2, 0), (3, 2, 1)), 14: ((2, 2, 0), (2, 2, 1)),
 }
 HALF = OWN // 2
 PARTS = ((0, OWN), (OWN, BLOCK - OWN))
@@ -80,7 +76,7 @@
 def kernel(
     latent, context, cond, gain, mod_shift, mod_scale, mod_gate, w_query, w_key, w_value, w_out, lambdas,
     context_bias, head_gain, out,
-    lat, ctx, mod, wqkv, part, msg, msg2, mods, qv, kvown, qown, kv, qb, qm, vctx, sscr, tops, acc, peak, nsend, nrm,
+    lat, ctx, hctx, mod, wqkv, part, msg, msg2, mods, qv, kvown, qown, kv, qb, qm, vctx, sscr, tops, acc, peak, nsend, nrm,
     wall, lsend, lrecv, wsend, wrecv, msend, mrecv, nsd, nrc, zsend, zqsend, kvrecv, qrecv, fsib, fplus, fminus,
     osend, orecv, local, ready,
 ):
@@ -110,7 +106,7 @@
             )
         )
     ]
-    for copy in loads:
+    for copy in loads[:4]:
         copy.start()
 
     cols = cond[:, pl.ds(pl.multiple_of(s * 128, 128), 128)]
@@ -125,6 +121,8 @@
                 line = index * 4 + r * 2 + half
                 msg[line : line + 1, :] = product[r : r + 1, half * 128 : half * 128 + 128]
     loads[3].wait()
+    for copy in loads[4:]:
+        copy.start()
     pl.semaphore_wait(barrier, 13)
 
     lcp = round_y(lat, ROWS, lsend, lrecv, s, y, c)
@@ -169,28 +167,30 @@
         normal = rows * lax.rsqrt(jnp.mean(rows * rows, axis=1, keepdims=True) + EPS)
         return (normal * (gain[...] * (1.0 + vector(1, r))) + vector(0, r)).astype(BF)
 
-    def project(p):
-        hidden = modulate(lat[p], 0)
-        rows = slice(PAIR * p, PAIR * p + PAIR)
+    def project(rows, p, more=None):
+        size = rows.shape[0]
+        hidden = modulate(rows, 0)
+        queries = jnp.dot(hidden, wqkv[0], preferred_element_type=F32).astype(BF)
+        if more is not None:
+            hidden = jnp.concatenate([hidden, more[...]], axis=0)
+        keys = jnp.dot(hidden, wqkv[1], preferred_element_type=F32).astype(BF)
+        values = jnp.dot(hidden, wqkv[2], preferred_element_type=F32)
         first = PAIR * p + HALF * (p // 2)
-        qv[0, rows, :] = jnp.dot(hidden, wqkv[0], preferred_element_type=F32)
-        keys = jnp.dot(hidden, wqkv[1], preferred_element_type=F32).astype(BF)
         for i in range(2):
-            kvown[i, first : first + PAIR, :] = keys[:, 128 * i : 128 * i + 128]
-        qv[1, rows, :] = jnp.dot(hidden, wqkv[2], preferred_element_type=F32)
+            columns = slice(128 * i, 128 * i + 128)
+            kvown[i, first : first + size, :] = keys[:size, columns]
+            for k in range(size // PAIR):
+                qown[p + k, i] = queries[PAIR * k : PAIR * k + PAIR, columns]
+            if more is not None:
+                kvown[i, 2 * OWN : 2 * OWN + CTXR, :] = keys[size:, columns]
+                kvown[i, 2 * OWN + CTXR : BLOCK, :] = values[size:, columns].astype(BF)
+        qv[PAIR * p : PAIR * p + size, :] = values[:size]
 
     for copy in loads[4:]:
         copy.wait()
-    hidden = modulate(ctx[...], 1)
-    keys = jnp.dot(hidden, wqkv[1], preferred_element_type=F32).astype(BF)
-    values = jnp.dot(hidden, wqkv[2], preferred_element_type=F32).astype(BF)
-    for i in range(2):
-        kvown[i, 2 * OWN : 2 * OWN + CTXR, :] = keys[:, 128 * i : 128 * i + 128]
-        kvown[i, 2 * OWN + CTXR : BLOCK, :] = values[:, 128 * i : 128 * i + 128]
     lcp[0].wait_recv()
-    project(0)
     lcp[7].wait_recv()
-    project(1)
+    project(lat[0:2].reshape(2 * PAIR, 2048), 0)
 
     primary = c == z // 2
     plus, minus = z * 4 + (x + 1) % 4, z * 4 + (x + 3) % 4
@@ -198,10 +198,9 @@
     def turn(part):
         for a in range(3 * part, 3 * part + 3):
             for i in range(2):
-                rows, columns = slice(128 * a, 128 * a + 128), slice(128 * i, 128 * i + 128)
-                qown[part, i, a % 3] = qv[0, rows, columns].T.astype(BF)
                 first = OWN * part + HALF + 128 * (a % 3)
-                kvown[i, first : first + 128, :] = qv[1, rows, columns].T.astype(BF)
+                block = qv[128 * a : 128 * a + 128, 128 * i : 128 * i + 128]
+                kvown[i, first : first + 128, :] = block.T.astype(BF)
 
     def distance(i):
         return (2 * c + i - z + 4) % 4
@@ -209,11 +208,27 @@
     def slot_of(dz):
         return 3 * (dz == 0).astype(jnp.int32) + (dz == 1).astype(jnp.int32) + 2 * (dz == 3).astype(jnp.int32)
 
-    def q_to(i, part):
-        slot = slot_of((z - 2 * c - i + 4) % 4)
+    def q_to(i, p):
+        rows = pl.ds(pl.multiple_of(PAIR * slot_of((z - 2 * c - i + 4) % 4), 16), PAIR)
         return remote(
-            qown.at[part, i], qb.at[slot], zqsend.at[i, part], qrecv.at[slot], (2 * c + i) * 4 + x, sib if part else t
+            qown.at[p, i], qb.at[p // 2, rows], zqsend.at[i, p], qrecv.at[p // 2, slot_of((z - 2 * c - i + 4) % 4)],
+            (2 * c + i) * 4 + x, sib if p % 2 else t,
         )
+
+    def send_q(p):
+        for i in range(2):
+            if p % 2:
+                q_to(i, p).start()
+                continue
+
+            @pl.when(distance(i) != 0)
+            def _():
+                q_to(i, p).start()
+
+            @pl.when(distance(i) == 0)
+            def _():
+                rows = qb.at[p // 2, 3 * PAIR : 4 * PAIR]
+                pltpu.make_async_copy(qown.at[p, i], rows, qrecv.at[p // 2, 3]).start()
 
     def part_of(ref, b, part):
         return ref.at[b, pl.ds(*PARTS[part])]
@@ -231,52 +246,42 @@
         b = source(dz, dx)
         src = part_of(kvown, z % 2, part) if (dz, dx) == (0, 0) else part_of(kv, b, part)
         dst = part_of(kv, b, part)
-        copies = []
+        copies = {}
         if dx == 0 or (dx == 3 and dz < 2):
-            copies.append(remote(src, dst, fplus.at[part, b], kvrecv.at[part, b], plus, t))
+            copies["p"] = remote(src, dst, fplus.at[part, b], kvrecv.at[part, b], plus, t)
         if dx == 0 or (dx == 1 and dz >= 2):
-            copies.append(remote(src, dst, fminus.at[part, b], kvrecv.at[part, b], minus, t))
-        copies.append(remote(src, dst, fsib.at[part, b], kvrecv.at[part, b], s, sib))
+            copies["m"] = remote(src, dst, fminus.at[part, b], kvrecv.at[part, b], minus, t)
+        copies["s"] = remote(src, dst, fsib.at[part, b], kvrecv.at[part, b], s, sib)
         return copies
 
     def arrive(b, part):
         pltpu.make_async_copy(part_of(kvown, 0, part), part_of(kv, b, part), kvrecv.at[part, b]).wait()
 
-    def pass_on(dz, dx, part, how):
-        if how < 2:
-            arrive(source(dz, dx), part)
-        for copy in onward(dz, dx, part):
-            if how == 0 or (how == 1) == (copy.device_id[1] is sib):
+    def go_on(dz, dx, part, ways="spm"):
+        for way, copy in onward(dz, dx, part).items():
+            if way in ways:
                 copy.start()
+
+    def pass_on(dz, dx, part, ways="spm"):
+        arrive(source(dz, dx), part)
+        go_on(dz, dx, part, ways)
 
     def send_part(part):
         for i in range(2):
-            if part:
-                q_to(i, 1).start()
-
-            @pl.when(distance(i) != 0)
-            def _():
-                if not part:
-                    q_to(i, 0).start()
 
             @pl.when(distance(i) == 0)
             def _():
-                if not part:
-                    pltpu.make_async_copy(qown.at[0, i], qb.at[3], qrecv.at[3]).start()
                 pltpu.make_async_copy(part_of(kvown, i, part), part_of(kv, s, part), kvrecv.at[part, s]).start()
 
         @pl.when(primary)
         def _():
-            for copy in onward(0, 0, part):
-                copy.start()
-
-        if part:
-            for i in range(2):
-
-                @pl.when(distance(i) % 2 == 1)
-                def _():
-                    kv_to(i, 0).start()
-                    kv_to(i, 1).start()
+            go_on(0, 0, part)
+
+        for i in range(2):
+
+            @pl.when(distance(i) % 2 == 1)
+            def _():
+                kv_to(i, part).start()
 
     def send_far(part):
         for i in range(2):
@@ -285,15 +290,20 @@
             def _():
                 kv_to(i, part).start()
 
+    send_q(0)
+    send_q(1)
     turn(0)
     send_part(0)
     lcp[5].wait_recv()
     lcp[6].wait_recv()
     lcp[9].start()
     lcp[8].wait_recv()
-    project(2)
+    project(lat[2], 2)
+    send_q(2)
+    hctx[...] = modulate(ctx[...], 1)
     lcp[9].wait_recv()
-    project(3)
+    project(lat[3], 3, hctx)
+    send_q(3)
     turn(1)
     send_part(1)
     wcp = round_y(wall, 256, wsend, wrecv, s, y, c)
@@ -303,17 +313,26 @@
     for u in range(UNITS):
         acc[u] = jnp.zeros_like(acc[u])
         peak[u] = jnp.full_like(peak[u], -1e30)
-    for k in range(4):
-        pltpu.make_async_copy(qown.at[0, 0], qb.at[k], qrecv.at[k]).wait()
-
-    for chunk in range(12):
-        tile, columns = chunk // 2, slice(128 * (chunk % 2), 128 * (chunk % 2) + 128)
-        block = qb[chunk // 3, chunk % 3]
-        zero = jnp.zeros((64, 128), BF)
-        qm[0, tile, 0:64, columns] = block[0:64]
-        qm[0, tile, 64:128, columns] = zero
-        qm[1, tile, 0:64, columns] = zero
-        qm[1, tile, 64:128, columns] = block[64:128]
+
+    @pl.when(primary)
+    def _():
+        pass_on(0, 1, 0)
+        pass_on(0, 3, 0)
+
+    def take_queries(part):
+        for k in range(4):
+            rows = qb.at[part, PAIR * k : PAIR * k + PAIR]
+            pltpu.make_async_copy(qown.at[0, 0], rows, qrecv.at[part, k]).wait()
+        for r in range(6):
+            tile, columns = 3 * part + r // 2, slice(128 * (r % 2), 128 * (r % 2) + 128)
+            block = qb[part, 128 * r : 128 * r + 128, :].astype(F32).T.astype(BF)
+            zero = jnp.zeros((64, 128), BF)
+            qm[0, tile, 0:64, columns] = block[0:64]
+            qm[0, tile, 64:128, columns] = zero
+            qm[1, tile, 0:64, columns] = zero
+            qm[1, tile, 64:128, columns] = block[64:128]
+
+    take_queries(0)
 
     def score(u, at, keys, size):
         raw = jnp.dot(keys, qm[u % 2, u // 2], preferred_element_type=F32)
@@ -331,51 +350,91 @@
         probs = jnp.exp2(sscr[slot, 0:size, :] * SCALE - shift).astype(BF)
         acc[u] = acc[u] * faded + jnp.dot(lhs, probs, preferred_element_type=F32)
 
-    def latent_keys(b):
-        return jnp.concatenate([kv[b, 0:HALF, :], kv[b, OWN : OWN + HALF, :]], axis=0)
-
-    def latent_lhs(b):
-        lhs = jnp.concatenate([kv[b, k : k + 128, :] for a in (HALF, OWN + HALF) for k in range(a, a + HALF, 128)], axis=1)
-        return jnp.concatenate([lhs, jnp.ones((16, OWN), BF)], axis=0)
-
-    def block_at(n):
+    def parts_of(n):
+        if isinstance(n, int):
+            pair = source(*FIRST[n]), source(*SECOND[n])
+            return *pair, OWN if n in (3, 4) else 0, 0 if n in (1, 2) else OWN
         late = (n >= 8).astype(jnp.int32)
         by = 2 * (n - 8 * late)
-        dz = ((PACKED[0] * (1 - late) + PACKED[1] * late) >> by) % 4
-        dx = ((PACKED[2] * (1 - late) + PACKED[3] * late) >> by) % 4
-        return source(dz, dx)
-
-    arrive(s, 0)
-    arrive(s, 1)
-    keys, lhs = latent_keys(s), latent_lhs(s)
-    for u in range(AHEAD):
-        score(u, u, keys, OWN)
-    for u in range(UNITS):
-        if u + AHEAD < UNITS:
-            score(u + AHEAD, u + AHEAD, keys, OWN)
-        weigh(u, u, lhs, OWN, None)
-
-
-    @pl.when(primary)
-    def _():
-        for place in PASS[0]:
-            pass_on(*place)
+        dz, dx, ez, ex = (((w[0] * (1 - late) + w[1] * late) >> by) % 4 for w in PACKED)
+        return source(dz, dx), source(ez, ex), OWN * (n < 5).astype(jnp.int32)
+
+    def rows_of(b, row, offset):
+        if not isinstance(row, int):
+            row = pl.multiple_of(row, 128)
+        return kv[b, pl.ds(row + offset, HALF), :]
+
+    def latent_keys(a, b, p, q):
+        return jnp.concatenate([rows_of(a, p, 0), rows_of(b, q, 0)], axis=0)
+
+    def latent_lhs(a, b, p, q):
+        halves = rows_of(a, p, HALF), rows_of(b, q, HALF)
+        lhs = jnp.concatenate([half[128 * k : 128 * k + 128] for half in halves for k in range(3)], axis=1)
+        return jnp.concatenate([lhs, jnp.ones((16, OWN), BF)], axis=0)
+
+    def stream(turns, keys, lhs, at=0, done=0, sizes=None, biases=None, after=None, ends=()):
+        size = lambda which: OWN if sizes is None else sizes[which]
+        for k in range(done, AHEAD):
+            which, u = turns[k]
+            score(u, at + k, keys[which], size(which))
+        coming = list(turns) + list(ends)
+        for k, (which, u) in enumerate(turns):
+            if k + AHEAD < len(coming):
+                other, v = coming[k + AHEAD]
+                score(v, at + k + AHEAD, keys[other], size(other))
+            weigh(u, at + k, lhs[which], size(which), None if biases is None else biases[which])
+            if after is not None:
+                after(which, u)
 
     @pl.when(jnp.logical_not(primary))
     def _():
         arrive(source(0, 1), 0)
+        arrive(source(0, 3), 0)
+
+    arrive(s, 0)
+    arrive(s, 1)
+    held = [parts_of(n) for n in range(4)]
+    keys, lhs = [latent_keys(*h) for h in held[:2]], [latent_lhs(*h) for h in held[:2]]
+    stream([(n, u) for n in range(2) for u in range(6)], keys, lhs)
+    both = primary, jnp.logical_not(primary)
+
+    @pl.when(both[0])
+    def _():
+        pass_on(1, 0, 0)
+        pass_on(3, 0, 0, "sm")
+
+    @pl.when(both[1])
+    def _():
+        arrive(source(1, 0), 0)
+        arrive(source(3, 0), 0)
+
+    stream([(0, u) for u in range(6)], [latent_keys(*held[2])], [latent_lhs(*held[2])])
+
+    @pl.when(both[0])
+    def _():
+        pass_on(0, 3, 1)
+        pass_on(0, 1, 1)
+        go_on(3, 0, 0, "p")
+
+    @pl.when(both[1])
+    def _():
         arrive(source(0, 1), 1)
-
-    keys = latent_keys(source(0, 1))
-    for u in range(AHEAD):
-        score(u, u, keys, OWN)
-
-    def step(n, b):
-        following = block_at(n + 1)
+        arrive(source(0, 3), 1)
+
+    send_far(0)
+    send_far(1)
+    take_queries(1)
+    keys, lhs = [latent_keys(*h) for h in held], [latent_lhs(*h) for h in held[:3]]
+    stream(
+        [(n, u) for n in range(3) for u in range(6, UNITS)], keys, lhs, at=2, ends=[(3, u) for u in range(AHEAD)]
+    )
+
+    def step(n, now):
+        following = parts_of(n + 1)
 
         @pl.when(primary)
         def _():
-            for steps in ((1, 2, 4), (5, 6, 7), (8, 10, 11), (12, 14)):
+            for steps in ((3, 4, 5), (6, 7, 8), (10, 11, 12), (13, 14)):
 
                 @pl.when((n >= steps[0]) & (n <= steps[-1]))
                 def _():
@@ -388,15 +447,17 @@
 
         @pl.when(jnp.logical_not(primary))
         def _():
-            arrive(following, 0)
-            arrive(following, 1)
-
-        @pl.when(n == 1)
-        def _():
-            send_far(0)
-            send_far(1)
-
-        @pl.when(n == 7)
+            @pl.when(n == 3)
+            def _():
+                arrive(following[0], 1)
+
+            @pl.when(n != 3)
+            def _():
+                arrive(following[0], 0)
+
+            arrive(following[1], 1)
+
+        @pl.when(n == 9)
         def _():
             for k in (1, 2):
                 wcp[k].wait_recv()
@@ -405,22 +466,16 @@
                 wcp[k].wait_recv()
                 wcp[k + 4].start()
 
-        @pl.when(n == 13)
-        def _():
-            wcp[5].wait_recv()
-            wcp[6].wait_recv()
-            wcp[9].start()
-
-        keys, later, lhs = latent_keys(b), latent_keys(following), latent_lhs(b)
-        for u in range(UNITS):
-            if u + AHEAD < UNITS:
-                score(u + AHEAD, u + AHEAD, keys, OWN)
-            else:
-                score(u + AHEAD - UNITS, u + AHEAD, later, OWN)
-            weigh(u, u, lhs, OWN, None)
+        stream(
+            [(0, u) for u in range(UNITS)], [latent_keys(*now, OWN), latent_keys(*following, OWN)], [latent_lhs(*now, OWN)],
+            done=AHEAD, ends=[(1, u) for u in range(AHEAD)],
+        )
         return following
 
-    last = lax.fori_loop(1, 15, step, source(0, 1))
+    last = lax.fori_loop(3, 15, step, (*held[3][:2], jnp.int32(OWN)))
+    wcp[5].wait_recv()
+    wcp[6].wait_recv()
+    wcp[9].start()
 
     lane = lax.broadcasted_iota(jnp.int32, (1, 128), 1)
     owner = y * 2 + z // 2
@@ -433,30 +488,27 @@
     half = 1 - primary.astype(jnp.int32)
 
     def piece(k):
-        offset = half if k % 4 // 2 == 0 else 3 * half + 3
+        offset = 3 * half if k < 8 else 1 + half
         target = ((y + offset) % 4) * 2 + k % 2
         src = nsend.at[ROWS * k : ROWS * k + ROWS]
-        return remote(src, nrm.at[head], osend.at[k], orecv.at[head], ((z + (2, 1, 3, 0)[k // 4]) % 4) * 4 + x, target)
+        return remote(src, nrm.at[head], osend.at[k], orecv.at[head], ((z + (2, 1, 3, 0)[k % 8 // 2]) % 4) * 4 + x, target)
 
     for k in range(8):
         pair = jnp.concatenate([kv[2 * k, 2 * OWN + CTXR : BLOCK, :], kv[2 * k + 1, 2 * OWN + CTXR : BLOCK, :]], axis=0)
         vctx[:, 128 * k : 128 * k + 128] = pair.astype(F32).T.astype(BF)
     size = 16 * CTXR
-    keys = (latent_keys(last), jnp.concatenate([kv[k, 2 * OWN : 2 * OWN + CTXR, :] for k in range(16)], axis=0))
-    lhs = (latent_lhs(last), jnp.concatenate([vctx[...], jnp.ones((16, size), BF)], axis=0))
-    sizes, biases = (OWN, size), (None, bias)
+    whole = source(*FIRST[15]), source(*FIRST[15]), 0, OWN
+    keys = (latent_keys(*whole), jnp.concatenate([kv[k, 2 * OWN : 2 * OWN + CTXR, :] for k in range(16)], axis=0))
+    lhs = (latent_lhs(*whole), jnp.concatenate([vctx[...], jnp.ones((16, size), BF)], axis=0))
     turns = [(0, u) for u in range(4)]
     for u in range(0, UNITS, 2):
         turns += [(1, u), (1, u + 1)]
         turns += [(0, u + 4), (0, u + 5)] if u + 5 < UNITS else []
-    pieces = 0
-    for k, (which, u) in enumerate(turns):
-        if k + AHEAD < len(turns):
-            other, v = turns[k + AHEAD]
-            score(v, k + AHEAD, keys[other], sizes[other])
-        weigh(u, k, lhs[which], sizes[which], biases[which])
+    sent = {2: range(0, 8), 4: range(8, 13), 5: range(13, 16)}
+
+    def finish(which, u):
         if which == 0 or u % 2 == 0:
-            continue
+            return
         tile = u // 2
         one, two = acc[2 * tile], acc[2 * tile + 1]
         mixed = one[0:128] / one[128:129] - lam * (two[0:128] / two[128:129])
@@ -465,14 +517,11 @@
             block = normed[:, 128 * r : 128 * r + 128].T * head_gain[...]
             row = QT * tile + 128 * r
             nsend[row : row + 128, :] = block.astype(BF)
-        if tile in (0, 2):
-            continue
-        ready = QT * (tile + 1) // ROWS
-        for e in range(pieces, ready):
-            if e not in (12, 13):
+        for e in sent.get(tile, ()):
+            if e not in (6, 7):
                 piece(e).start()
                 continue
-            mine = primary & (c == e - 12)
+            mine = primary & (c == e - 6)
 
             @pl.when(mine)
             def _():
@@ -483,7 +532,7 @@
             def _():
                 piece(e).start()
 
-        pieces = ready
+    stream(turns, keys, lhs, done=AHEAD, sizes=(OWN, size), biases=(None, bias), after=finish)
 
     for k in (0, 7, 8, 9):
         wcp[k].wait_recv()
@@ -504,27 +553,29 @@
     for copy in lcp + wcp + mcp + ncp:
         copy.wait_send()
     for i in range(2):
-        q_to(i, 1).wait_send()
+        for p in (1, 3):
+            q_to(i, p).wait_send()
 
         @pl.when(distance(i) != 0)
         def _():
-            q_to(i, 0).wait_send()
+            for p in (0, 2):
+                q_to(i, p).wait_send()
             for part in range(2):
                 kv_to(i, part).wait_send()
 
     @pl.when(primary)
     def _():
-        for place in ORDER:
+        for place in [(dz, dx) for dz in range(4) for dx in range(4)]:
             for part in range(2):
-                for copy in onward(*place, part):
+                for copy in onward(*place, part).values():
                     copy.wait_send()
 
     for e in range(16):
-        if e not in (12, 13):
+        if e not in (6, 7):
             piece(e).wait_send()
             continue
 
-        @pl.when(jnp.logical_not(primary & (c == e - 12)))
+        @pl.when(jnp.logical_not(primary & (c == e - 6)))
         def _():
             piece(e).wait_send()
 
@@ -545,17 +596,18 @@
         scratch_shapes=[
             pltpu.VMEM((4, PAIR, 2048), BF),
             pltpu.VMEM((CTXR, 2048), BF),
+            pltpu.VMEM((CTXR, 2048), BF),
             pltpu.VMEM((3, 128, 256), BF),
             pltpu.VMEM((3, 2048, 256), BF),
             pltpu.VMEM((16, 16, 128), F32),
             pltpu.VMEM((16, 128), F32),
             pltpu.VMEM((16, 128), F32),
             pltpu.VMEM((8, 16, 128), F32),
-            pltpu.VMEM((2, OWN, 256), F32),
+            pltpu.VMEM((OWN, 256), F32),
             pltpu.VMEM((2, BLOCK, 128), BF),
-            pltpu.VMEM((2, 2, 3, 128, 128), BF),
+            pltpu.VMEM((4, 2, PAIR, 128), BF),
             pltpu.VMEM((16, BLOCK, 128), BF),
-            pltpu.VMEM((4, 3, 128, 128), BF),
+            pltpu.VMEM((2, OWN, 128), BF),
             pltpu.VMEM((2, NQ, 128, QT), BF),
             pltpu.VMEM((128, 16 * CTXR), BF),
             pltpu.VMEM((AHEAD + 1, 16 * CTXR, QT), F32),
@@ -567,7 +619,7 @@
             pltpu.VMEM((4, 512, 2048), BF),
             dma((10,)), dma((10,)), dma((10,)), dma((10,)),
             dma((16,)), dma((16,)), dma((8,)), dma((8,)),
-            dma((2, 2)), dma((2, 2)), dma((2, 16)), dma((4,)),
+            dma((2, 2)), dma((2, 4)), dma((2, 16)), dma((2, 4)),
             dma((2, 16)), dma((2, 16)), dma((2, 16)),
             dma((16,)), dma((16,)), dma((9,)),
             pltpu.SemaphoreType.REGULAR,

time: 87.4 us -> 84.3 us (0.965)
  Pallas kernels: 85.4 us -> 82.4 us
    pallas_call x1, Pallas kernels: 85.4 us -> 82.4 us  [per_device(): pl.pallas_call(kernel, name='block', out_shape=jax.ShapeDtypeStruct(laten...]
where the time goes in v5:
time: 84.3 us; the launch traced here: 84.1 us
  Pallas kernels  82.4 us (98%)
  local copies, waits for them, and re-layouts  1.77 us (2%)
    pallas_call x1, Pallas kernels, per_device(): pl.pallas_call(kernel, name='block', out_shape=jax.ShapeDtypeStruct(laten...  82.4 us
    unnamed x1, local copies, waits for them, and re-layouts  1.77 us

profile of v5, /device:TPU:1, one launch (start us, length us, event | category | flops | bytes accessed | tf_op | source)
XLA Modules:
  0.0 84.1 jit_solution(10549449673117705048)
XLA Ops:
  0.0 82.4 %block.1 = bf16[96,2048]{1,0:T(8,128)(2,1)} custom-call(bf16[96,2048]{1,0:T(8,128)(2,1)} %latent.1, bf16[64,2048]{1,0:T(8,128)(2,1)} %context.1, f32[2,2048]{1,0:T(2,128)} %cond.1, f32[1,2048]{1,0:T(1,128)} %bitcast.4, bf16[128,256]{1,0:T(8,128)(2,1)} %mod_shift.1, bf16[128,256]{1,0:T(8,128)(2,1)} %mod_scale.1, bf16[128,256]{1,0:T(8,128)(2,1)} %mod_gate.1, ...), custom_call_target="tpu_custom_call" | custom-call | tf_op jit(solution)/shard_map/block/pallas_call | solution.py:590
  82.4 1.8 %copy.16 = bf16[96,2048]{1,0:T(8,128)(2,1)} copy(bf16[96,2048]{1,0:T(8,128)(2,1)} %block.1) | data formatting | bytes 786432

commit v6 on v5

--- a/solution.py
+++ b/solution.py
@@ -48,6 +48,10 @@
     )
 
 
+def settle(ref, sem):
+    pltpu.make_async_copy(ref, ref, sem).wait()
+
+
 def round_y(buf, rows, send, recv, s, y, c):
     up, down = ((y + 1) % 4) * 2 + c, ((y + 3) % 4) * 2 + c
     sib = y * 2 + 1 - c
@@ -74,10 +78,10 @@
 
 
 def kernel(
-    latent, context, cond, gain, mod_shift, mod_scale, mod_gate, w_query, w_key, w_value, w_out, lambdas,
-    context_bias, head_gain, out,
+    latent, context, cond_in, gain_in, mod_shift, mod_scale, mod_gate, w_query, w_key, w_value, w_out, lambdas_in,
+    bias_in, head_gain_in, out,
     lat, ctx, hctx, mod, wqkv, part, msg, msg2, mods, qv, kvown, qown, kv, qb, qm, vctx, sscr, tops, acc, peak, nsend, nrm,
-    wall, lsend, lrecv, wsend, wrecv, msend, mrecv, nsd, nrc, zsend, zqsend, kvrecv, qrecv, fsib, fplus, fminus,
+    wall, cond, gain, lambdas, context_bias, head_gain, lsend, lrecv, wsend, wrecv, msend, mrecv, nsd, nrc, zsend, zqsend, kvrecv, qrecv, fwd,
     osend, orecv, local, ready,
 ):
     s, t = lax.axis_index("sp"), lax.axis_index("tp")
@@ -94,11 +98,16 @@
         pltpu.make_async_copy(src, dst, local.at[k])
         for k, (src, dst) in enumerate(
             (
+                (cond_in, cond),
                 (mod_shift, mod.at[0]),
                 (mod_scale, mod.at[1]),
                 (mod_gate, mod.at[2]),
                 (latent, lat.at[0, pl.ds(pl.multiple_of(c * ROWS, 16), ROWS)]),
                 (context, ctx),
+                (lambdas_in, lambdas),
+                (bias_in, context_bias),
+                (gain_in, gain),
+                (head_gain_in, head_gain),
                 (w_query, wqkv.at[0]),
                 (w_key, wqkv.at[1]),
                 (w_value, wqkv.at[2]),
@@ -106,22 +115,23 @@
             )
         )
     ]
-    for copy in loads[:4]:
+    for copy in loads[:5]:
         copy.start()
+    loads[0].wait()
 
     cols = cond[:, pl.ds(pl.multiple_of(s * 128, 128), 128)]
     activated = (cols / (1.0 + jnp.exp(-cols))).astype(BF)
     activated = jnp.concatenate([activated.astype(F32), jnp.zeros((6, 128), F32)], axis=0).astype(BF)
     msg[12:16, :] = jnp.zeros((4, 128), F32)
     for index in range(3):
-        loads[index].wait()
+        loads[index + 1].wait()
         product = jnp.dot(activated, mod[index], preferred_element_type=F32)
         for r in range(2):
             for half in range(2):
                 line = index * 4 + r * 2 + half
                 msg[line : line + 1, :] = product[r : r + 1, half * 128 : half * 128 + 128]
-    loads[3].wait()
-    for copy in loads[4:]:
+    loads[4].wait()
+    for copy in loads[5:]:
         copy.start()
     pl.semaphore_wait(barrier, 13)
 
@@ -131,19 +141,20 @@
     for d in range(1, 4):
         pl.semaphore_signal(ready, inc=1, device_id=((z + d) % 4 * 4 + x, t), device_id_type=MESH)
     pl.semaphore_wait(ready, 3)
-    mcp = [remote(msg, part.at[s], msend.at[d], mrecv.at[d], (s + d) % 16, t) for d in range(1, 16)]
+    mcp = [remote(msg, part.at[s], msend.at[0], mrecv.at[0], (s + d) % 16, t) for d in range(1, 16)]
     for copy in mcp:
         copy.start()
     part[s] = msg[...]
-    for copy in mcp:
-        copy.wait_recv()
+    settle(part.at[0:15], mrecv.at[0])
     total = part[0]
     for k in range(1, 16):
         total = total + part[k]
+    for copy in loads[5:]:
+        copy.wait()
     msg2[...] = total
     msg2[12:13, 0:2] = lambdas[...]
     msg2[13:14, 0:2] = context_bias[...]
-    ncp = [remote(msg2, mods.at[t], nsd.at[d], nrc.at[d], s, (t + d) % 8) for d in range(1, 8)]
+    ncp = [remote(msg2, mods.at[t], nsd.at[0], nrc.at[0], s, (t + d) % 8) for d in range(1, 8)]
     for copy in ncp:
         copy.start()
     mods[t] = msg2[...]
@@ -155,8 +166,7 @@
     lcp[7].start()
     lcp[4].wait_recv()
     lcp[8].start()
-    for copy in ncp:
-        copy.wait_recv()
+    settle(mods.at[0:7], nrc.at[0])
 
     def vector(index, r):
         row = index * 4 + r * 2
@@ -186,8 +196,6 @@
                 kvown[i, 2 * OWN + CTXR : BLOCK, :] = values[size:, columns].astype(BF)
         qv[PAIR * p : PAIR * p + size, :] = values[:size]
 
-    for copy in loads[4:]:
-        copy.wait()
     lcp[0].wait_recv()
     lcp[7].wait_recv()
     project(lat[0:2].reshape(2 * PAIR, 2048), 0)
@@ -211,7 +219,7 @@
     def q_to(i, p):
         rows = pl.ds(pl.multiple_of(PAIR * slot_of((z - 2 * c - i + 4) % 4), 16), PAIR)
         return remote(
-            qown.at[p, i], qb.at[p // 2, rows], zqsend.at[i, p], qrecv.at[p // 2, slot_of((z - 2 * c - i + 4) % 4)],
+            qown.at[p, i], qb.at[p // 2, rows], zqsend.at[i, p], qrecv.at[p // 2],
             (2 * c + i) * 4 + x, sib if p % 2 else t,
         )
 
@@ -228,7 +236,7 @@
             @pl.when(distance(i) == 0)
             def _():
                 rows = qb.at[p // 2, 3 * PAIR : 4 * PAIR]
-                pltpu.make_async_copy(qown.at[p, i], rows, qrecv.at[p // 2, 3]).start()
+                pltpu.make_async_copy(qown.at[p, i], rows, qrecv.at[p // 2]).start()
 
     def part_of(ref, b, part):
         return ref.at[b, pl.ds(*PARTS[part])]
@@ -248,10 +256,10 @@
         dst = part_of(kv, b, part)
         copies = {}
         if dx == 0 or (dx == 3 and dz < 2):
-            copies["p"] = remote(src, dst, fplus.at[part, b], kvrecv.at[part, b], plus, t)
+            copies["p"] = remote(src, dst, fwd.at[0], kvrecv.at[part, b], plus, t)
         if dx == 0 or (dx == 1 and dz >= 2):
-            copies["m"] = remote(src, dst, fminus.at[part, b], kvrecv.at[part, b], minus, t)
-        copies["s"] = remote(src, dst, fsib.at[part, b], kvrecv.at[part, b], s, sib)
+            copies["m"] = remote(src, dst, fwd.at[1], kvrecv.at[part, b], minus, t)
+        copies["s"] = remote(src, dst, fwd.at[2], kvrecv.at[part, b], s, sib)
         return copies
 
     def arrive(b, part):
@@ -320,9 +328,7 @@
         pass_on(0, 3, 0)
 
     def take_queries(part):
-        for k in range(4):
-            rows = qb.at[part, PAIR * k : PAIR * k + PAIR]
-            pltpu.make_async_copy(qown.at[0, 0], rows, qrecv.at[part, k]).wait()
+        settle(qb.at[part], qrecv.at[part])
         for r in range(6):
             tile, columns = 3 * part + r // 2, slice(128 * (r % 2), 128 * (r % 2) + 128)
             block = qb[part, 128 * r : 128 * r + 128, :].astype(F32).T.astype(BF)
@@ -487,11 +493,16 @@
     head = y * 4 + z
     half = 1 - primary.astype(jnp.int32)
 
+    def spot(h, row):
+        return 8 * (h % 4 // 2 == row // 2).astype(jnp.int32) + h // 4 * 2 + h % 2
+
     def piece(k):
         offset = 3 * half if k < 8 else 1 + half
         target = ((y + offset) % 4) * 2 + k % 2
         src = nsend.at[ROWS * k : ROWS * k + ROWS]
-        return remote(src, nrm.at[head], osend.at[k], orecv.at[head], ((z + (2, 1, 3, 0)[k % 8 // 2]) % 4) * 4 + x, target)
+        row = (z + (2, 1, 3, 0)[k % 8 // 2]) % 4
+        late = (row // 2 == z // 2).astype(jnp.int32)
+        return remote(src, nrm.at[spot(head, row)], osend.at[0], orecv.at[late], row * 4 + x, target)
 
     for k in range(8):
         pair = jnp.concatenate([kv[2 * k, 2 * OWN + CTXR : BLOCK, :], kv[2 * k + 1, 2 * OWN + CTXR : BLOCK, :]], axis=0)
@@ -526,7 +537,7 @@
             @pl.when(mine)
             def _():
                 src = nsend.at[ROWS * e : ROWS * e + ROWS]
-                pltpu.make_async_copy(src, nrm.at[head], orecv.at[head]).start()
+                pltpu.make_async_copy(src, nrm.at[spot(head, z)], orecv.at[1]).start()
 
             @pl.when(jnp.logical_not(mine))
             def _():
@@ -537,12 +548,10 @@
     for k in (0, 7, 8, 9):
         wcp[k].wait_recv()
     attended = jnp.zeros((ROWS, 2048), F32)
-    for k in (1 - z // 2, z // 2):
-        firsts = [4 * ((y + off) % 4) + 2 * k for off in (0, 3, 1, 2)]
-        for first in firsts:
-            for h in (first, first + 1):
-                pltpu.make_async_copy(nsend.at[0:ROWS], nrm.at[h], orecv.at[h]).wait()
-        for p, first in enumerate(firsts):
+    for late, k in enumerate((1 - z // 2, z // 2)):
+        settle(nrm.at[8 * late : 8 * late + 8], orecv.at[late])
+        for p, off in enumerate((0, 3, 1, 2)):
+            first = 8 * late + 2 * ((y + off) % 4)
             rows = jnp.concatenate([nrm[first], nrm[first + 1]], axis=1)
             part_of_w = wall[p, pl.ds(pl.multiple_of(256 * k, 256), 256), :]
             product = jnp.dot(rows, part_of_w, preferred_element_type=F32)
@@ -550,8 +559,10 @@
     rows = lat[0, pl.ds(pl.multiple_of(c * ROWS, 16), ROWS), :].astype(F32)
     out[...] = (rows + vector(2, 0) * attended.astype(BF).astype(F32)).astype(BF)
 
-    for copy in lcp + wcp + mcp + ncp:
+    for copy in lcp + wcp:
         copy.wait_send()
+    settle(part.at[0:15], msend.at[0])
+    settle(mods.at[0:7], nsd.at[0])
     for i in range(2):
         for p in (1, 3):
             q_to(i, p).wait_send()
@@ -565,19 +576,17 @@
 
     @pl.when(primary)
     def _():
-        for place in [(dz, dx) for dz in range(4) for dx in range(4)]:
-            for part in range(2):
-                for copy in onward(*place, part).values():
-                    copy.wait_send()
-
-    for e in range(16):
-        if e not in (6, 7):
-            piece(e).wait_send()
-            continue
-
-        @pl.when(jnp.logical_not(primary & (c == e - 6)))
-        def _():
-            piece(e).wait_send()
+        settle(kv.at[0:6], fwd.at[0])
+        settle(kv.at[0:6], fwd.at[1])
+        settle(kv, fwd.at[2])
+
+    @pl.when(primary)
+    def _():
+        settle(nsend.at[0 : 15 * ROWS], osend.at[0])
+
+    @pl.when(jnp.logical_not(primary))
+    def _():
+        settle(nsend, osend.at[0])
 
 
 def per_device(
@@ -586,12 +595,12 @@
 ):
     dma = pltpu.SemaphoreType.DMA
     vmem = pl.BlockSpec(memory_space=pltpu.VMEM)
-    hbm = pl.BlockSpec(memory_space=pl.ANY)
+    hbm = pl.BlockSpec(memory_space=pltpu.HBM)
     return pl.pallas_call(
         kernel,
         name="block",
         out_shape=jax.ShapeDtypeStruct(latent.shape, BF),
-        in_specs=[hbm, hbm, vmem, vmem] + [hbm] * 7 + [vmem] * 3,
+        in_specs=[hbm] * 14,
         out_specs=vmem,
         scratch_shapes=[
             pltpu.VMEM((4, PAIR, 2048), BF),
@@ -617,11 +626,16 @@
             pltpu.VMEM((1536, 128), BF),
             pltpu.VMEM((16, ROWS, 128), BF),
             pltpu.VMEM((4, 512, 2048), BF),
+            pltpu.VMEM((2, 2048), F32),
+            pltpu.VMEM((1, 2048), F32),
+            pltpu.VMEM((1, 2), F32),
+            pltpu.VMEM((1, 2), F32),
+            pltpu.VMEM((1, 128), F32),
             dma((10,)), dma((10,)), dma((10,)), dma((10,)),
-            dma((16,)), dma((16,)), dma((8,)), dma((8,)),
-            dma((2, 2)), dma((2, 4)), dma((2, 16)), dma((2, 4)),
-            dma((2, 16)), dma((2, 16)), dma((2, 16)),
-            dma((16,)), dma((16,)), dma((9,)),
+            dma((1,)), dma((1,)), dma((1,)), dma((1,)),
+            dma((2, 2)), dma((2, 4)), dma((2, 16)), dma((2,)),
+            dma((3,)),
+            dma((1,)), dma((2,)), dma((14,)),
             pltpu.SemaphoreType.REGULAR,
         ],
         compiler_params=pltpu.CompilerParams(

time: 84.3 us -> 81.7 us (0.969)
  Pallas kernels: 82.4 us -> 79.8 us
    pallas_call x1, Pallas kernels: 82.4 us -> 79.8 us  [per_device(): pl.pallas_call(kernel, name='block', out_shape=jax.ShapeDtypeStruct(laten...]
where the time goes in v6:
time: 81.7 us; the launch traced here: 81.6 us
  Pallas kernels  79.8 us (98%)
  local copies, waits for them, and re-layouts  1.77 us (2%)
    pallas_call x1, Pallas kernels, per_device(): pl.pallas_call(kernel, name='block', out_shape=jax.ShapeDtypeStruct(laten...  79.8 us
    unnamed x1, local copies, waits for them, and re-layouts  1.77 us

profile of v6, /device:TPU:1, one launch (start us, length us, event | category | flops | bytes accessed | tf_op | source)
XLA Modules:
  0.0 81.6 jit_solution(11432253077145632923)
XLA Ops:
  0.0 79.8 %block.1 = bf16[96,2048]{1,0:T(8,128)(2,1)} custom-call(bf16[96,2048]{1,0:T(8,128)(2,1)} %latent.1, bf16[64,2048]{1,0:T(8,128)(2,1)} %context.1, f32[2,2048]{1,0:T(2,128)} %cond_in.1, f32[1,2048]{1,0:T(1,128)} %bitcast.4, bf16[128,256]{1,0:T(8,128)(2,1)} %mod_shift.1, bf16[128,256]{1,0:T(8,128)(2,1)} %mod_scale.1, bf16[128,256]{1,0:T(8,128)(2,1)} %mod_gate.1, ...), custom_call_target="tpu_custom_call" | custom-call | tf_op jit(solution)/shard_map/block/pallas_call | solution.py:599
  79.8 1.8 %copy.16 = bf16[96,2048]{1,0:T(8,128)(2,1)} copy(bf16[96,2048]{1,0:T(8,128)(2,1)} %block.1) | data formatting | bytes 786432

commit v7 on v6

--- a/solution.py
+++ b/solution.py
@@ -23,6 +23,7 @@
 NQ = 6
 UNITS = 12
 AHEAD = 3
+TURNS = (6, 7, 8, 9, 10, 11, 0, 1, 2, 3, 4, 5)
 FIRST = (
     (0, 0), (0, 1), (1, 0), (0, 1), (1, 0), (0, 2), (1, 1), (1, 3), (3, 1), (3, 3), (2, 0), (1, 2), (2, 1), (2, 3),
     (3, 2), (2, 2),
@@ -61,7 +62,7 @@
         return buf.at[slot, pl.ds(pl.multiple_of(c * rows + offset, 16), size)]
 
     def one(k, source, slot, offset, size, to):
-        return remote(at(source, offset, size), at(slot, offset, size), send.at[k], recv.at[k], s, to)
+        return remote(at(source, offset, size), at(slot, offset, size), send.at[(0, 1, 1, 1, 1, 2, 2, 0, 0, 0)[k]], recv.at[k], s, to)
 
     return [
         one(0, 0, 0, 0, rows, sib),
@@ -432,7 +433,7 @@
     take_queries(1)
     keys, lhs = [latent_keys(*h) for h in held], [latent_lhs(*h) for h in held[:3]]
     stream(
-        [(n, u) for n in range(3) for u in range(6, UNITS)], keys, lhs, at=2, ends=[(3, u) for u in range(AHEAD)]
+        [(n, u) for n in range(3) for u in range(6, UNITS)], keys, lhs, at=2, ends=[(3, u) for u in TURNS[:AHEAD]]
     )
 
     def step(n, now):
@@ -473,8 +474,8 @@
                 wcp[k + 4].start()
 
         stream(
-            [(0, u) for u in range(UNITS)], [latent_keys(*now, OWN), latent_keys(*following, OWN)], [latent_lhs(*now, OWN)],
-            done=AHEAD, ends=[(1, u) for u in range(AHEAD)],
+            [(0, u) for u in TURNS], [latent_keys(*now, OWN), latent_keys(*following, OWN)], [latent_lhs(*now, OWN)],
+            done=AHEAD, ends=[(1, u) for u in TURNS[:AHEAD]],
         )
         return following
 
@@ -511,11 +512,10 @@
     whole = source(*FIRST[15]), source(*FIRST[15]), 0, OWN
     keys = (latent_keys(*whole), jnp.concatenate([kv[k, 2 * OWN : 2 * OWN + CTXR, :] for k in range(16)], axis=0))
     lhs = (latent_lhs(*whole), jnp.concatenate([vctx[...], jnp.ones((16, size), BF)], axis=0))
-    turns = [(0, u) for u in range(4)]
-    for u in range(0, UNITS, 2):
-        turns += [(1, u), (1, u + 1)]
-        turns += [(0, u + 4), (0, u + 5)] if u + 5 < UNITS else []
-    sent = {2: range(0, 8), 4: range(8, 13), 5: range(13, 16)}
+    turns = [(0, u) for u in TURNS[:4]]
+    for k in range(0, UNITS, 2):
+        turns += [(1, u) for u in TURNS[k : k + 2]] + [(0, u) for u in TURNS[k + 4 : k + 6]]
+    sent = {5: range(8, 16), 0: range(0, 2), 1: range(2, 5), 2: range(5, 8)}
 
     def finish(which, u):
         if which == 0 or u % 2 == 0:
@@ -559,8 +559,10 @@
     rows = lat[0, pl.ds(pl.multiple_of(c * ROWS, 16), ROWS), :].astype(F32)
     out[...] = (rows + vector(2, 0) * attended.astype(BF).astype(F32)).astype(BF)
 
-    for copy in lcp + wcp:
-        copy.wait_send()
+    for ref, rows, sem in ((lat, ROWS, lsend), (wall, 256, wsend)):
+        settle(ref.at[0:2], sem.at[0])
+        settle(ref.at[0], sem.at[1])
+        settle(ref.at[0, 0:rows], sem.at[2])
     settle(part.at[0:15], msend.at[0])
     settle(mods.at[0:7], nsd.at[0])
     for i in range(2):
@@ -631,7 +633,7 @@
             pltpu.VMEM((1, 2), F32),
             pltpu.VMEM((1, 2), F32),
             pltpu.VMEM((1, 128), F32),
-            dma((10,)), dma((10,)), dma((10,)), dma((10,)),
+            dma((3,)), dma((10,)), dma((3,)), dma((10,)),
             dma((1,)), dma((1,)), dma((1,)), dma((1,)),
             dma((2, 2)), dma((2, 4)), dma((2, 16)), dma((2,)),
             dma((3,)),

time: 81.7 us -> 81.6 us (level)
  no operation moved by 1% of the time
where the time goes in v7:
time: 81.6 us; the launch traced here: 81.4 us
  Pallas kernels  79.7 us (98%)
  local copies, waits for them, and re-layouts  1.77 us (2%)
    pallas_call x1, Pallas kernels, per_device(): pl.pallas_call(kernel, name='block', out_shape=jax.ShapeDtypeStruct(laten...  79.7 us
    unnamed x1, local copies, waits for them, and re-layouts  1.77 us

profile of v7, /device:TPU:1, one launch (start us, length us, event | category | flops | bytes accessed | tf_op | source)
XLA Modules:
  0.0 81.4 jit_solution(13676265260632545544)
XLA Ops:
  0.0 79.7 %block.1 = bf16[96,2048]{1,0:T(8,128)(2,1)} custom-call(bf16[96,2048]{1,0:T(8,128)(2,1)} %latent.1, bf16[64,2048]{1,0:T(8,128)(2,1)} %context.1, f32[2,2048]{1,0:T(2,128)} %cond_in.1, f32[1,2048]{1,0:T(1,128)} %bitcast.4, bf16[128,256]{1,0:T(8,128)(2,1)} %mod_shift.1, bf16[128,256]{1,0:T(8,128)(2,1)} %mod_scale.1, bf16[128,256]{1,0:T(8,128)(2,1)} %mod_gate.1, ...), custom_call_target="tpu_custom_call" | custom-call | tf_op jit(solution)/shard_map/block/pallas_call | solution.py:601
  79.7 1.8 %copy.16 = bf16[96,2048]{1,0:T(8,128)(2,1)} copy(bf16[96,2048]{1,0:T(8,128)(2,1)} %block.1) | data formatting | bytes 786432

commit v8 on v7

--- a/solution.py
+++ b/solution.py
@@ -36,7 +36,8 @@
 )
 PASS = {
     3: ((1, 0, 1), (3, 0, 1)), 4: ((0, 2, 0), (0, 2, 1)), 5: ((1, 1, 0), (1, 1, 1)), 6: ((1, 3, 0), (1, 3, 1)),
-    7: ((2, 0, 0), (2, 0, 1), (3, 1, 0), (3, 1, 1)), 8: ((3, 3, 0), (3, 3, 1)), 10: ((1, 2, 0), (1, 2, 1)),
+    7: ((3, 1, 0, "s"), (3, 1, 1, "s"), (2, 0, 0), (2, 0, 1), (3, 1, 0, "m"), (3, 1, 1, "m")), 8: ((3, 3, 0), (3, 3, 1)),
+    10: ((1, 2, 0), (1, 2, 1)),
     11: ((2, 1, 0), (2, 1, 1)), 12: ((2, 3, 0), (2, 3, 1)), 13: ((3, 2, 0), (3, 2, 1)), 14: ((2, 2, 0), (2, 2, 1)),
 }
 HALF = OWN // 2
@@ -220,7 +221,7 @@
     def q_to(i, p):
         rows = pl.ds(pl.multiple_of(PAIR * slot_of((z - 2 * c - i + 4) % 4), 16), PAIR)
         return remote(
-            qown.at[p, i], qb.at[p // 2, rows], zqsend.at[i, p], qrecv.at[p // 2],
+            qown.at[p, i], qb.at[p // 2, rows], zqsend.at[2 if p % 2 else i], qrecv.at[p // 2],
             (2 * c + i) * 4 + x, sib if p % 2 else t,
         )
 
@@ -244,7 +245,7 @@
 
     def kv_to(i, part):
         return remote(
-            part_of(kvown, i, part), part_of(kv, s, part), zsend.at[i, part], kvrecv.at[part, s],
+            part_of(kvown, i, part), part_of(kv, s, part), zsend.at[i], kvrecv.at[part, s],
             (2 * c + i) * 4 + x, t,
         )
 
@@ -272,7 +273,8 @@
                 copy.start()
 
     def pass_on(dz, dx, part, ways="spm"):
-        arrive(source(dz, dx), part)
+        if "s" in ways:
+            arrive(source(dz, dx), part)
         go_on(dz, dx, part, ways)
 
     def send_part(part):
@@ -565,16 +567,13 @@
         settle(ref.at[0, 0:rows], sem.at[2])
     settle(part.at[0:15], msend.at[0])
     settle(mods.at[0:7], nsd.at[0])
+    settle(qb.at[0], zqsend.at[2])
     for i in range(2):
-        for p in (1, 3):
-            q_to(i, p).wait_send()
 
         @pl.when(distance(i) != 0)
         def _():
-            for p in (0, 2):
-                q_to(i, p).wait_send()
-            for part in range(2):
-                kv_to(i, part).wait_send()
+            settle(qb.at[0, 0 : 2 * PAIR], zqsend.at[i])
+            settle(kv.at[0], zsend.at[i])
 
     @pl.when(primary)
     def _():
@@ -635,7 +634,7 @@
             pltpu.VMEM((1, 128), F32),
             dma((3,)), dma((10,)), dma((3,)), dma((10,)),
             dma((1,)), dma((1,)), dma((1,)), dma((1,)),
-            dma((2, 2)), dma((2, 4)), dma((2, 16)), dma((2,)),
+            dma((2,)), dma((3,)), dma((2, 16)), dma((2,)),
             dma((3,)),
             dma((1,)), dma((2,)), dma((14,)),
             pltpu.SemaphoreType.REGULAR,

time: 81.6 us -> 81.6 us (level)
  no operation moved by 1% of the time
where the time goes in v8:
time: 81.6 us; the launch traced here: 81.4 us
  Pallas kernels  79.6 us (98%)
  local copies, waits for them, and re-layouts  1.77 us (2%)
    pallas_call x1, Pallas kernels, per_device(): pl.pallas_call(kernel, name='block', out_shape=jax.ShapeDtypeStruct(laten...  79.6 us
    unnamed x1, local copies, waits for them, and re-layouts  1.77 us

profile of v8, /device:TPU:1, one launch (start us, length us, event | category | flops | bytes accessed | tf_op | source)
XLA Modules:
  0.0 81.4 jit_solution(15000608959746153120)
XLA Ops:
  0.0 79.6 %block.1 = bf16[96,2048]{1,0:T(8,128)(2,1)} custom-call(bf16[96,2048]{1,0:T(8,128)(2,1)} %latent.1, bf16[64,2048]{1,0:T(8,128)(2,1)} %context.1, f32[2,2048]{1,0:T(2,128)} %cond_in.1, f32[1,2048]{1,0:T(1,128)} %bitcast.4, bf16[128,256]{1,0:T(8,128)(2,1)} %mod_shift.1, bf16[128,256]{1,0:T(8,128)(2,1)} %mod_scale.1, bf16[128,256]{1,0:T(8,128)(2,1)} %mod_gate.1, ...), custom_call_target="tpu_custom_call" | custom-call | tf_op jit(solution)/shard_map/block/pallas_call | solution.py:600
  79.6 1.8 %copy.16 = bf16[96,2048]{1,0:T(8,128)(2,1)} copy(bf16[96,2048]{1,0:T(8,128)(2,1)} %block.1) | data formatting | bytes 786432
